TPU v7x, 128 devices: a whole 4x4x4 slice. The times are simulated.
128 devices in a mesh: sp: 16 (over z, y), tp: 8 (over x, core).
Axes of the slice: x: 4, y: 4, z: 4, core: 2. Of those that a mesh axis runs over, the one named last changes fastest.
Arguments:
- residual_in: bfloat16 [12288, 2048], P('sp', 'tp'), may hold values from -11 to 11
- queries: bfloat16 [12288, 1024], P('sp', 'tp'), may hold values from -6 to 6
- keys: bfloat16 [12288, 256], P('sp'), may hold values from -6 to 6
- values: bfloat16 [12288, 256], P('sp'), may hold values from -6 to 6
- query_gain: float32 [128], replicated, may hold values from 1.5 to 5
- key_norm_gain: float32 [128], replicated, may hold values from 1.5 to 5
- out_weight: bfloat16 [1024, 2048], P('tp'), may hold values from -0.1875 to 0.1875
- mlp_gain: float32 [2048], replicated, may hold values from 0.1 to 1.9
- gate_weight: bfloat16 [2048, 5632], P('sp', 'tp'), may hold values from -0.125 to 0.125
- up_weight: bfloat16 [2048, 5632], P('sp', 'tp'), may hold values from -0.125 to 0.125
- down_weight: bfloat16 [5632, 2048], P('tp', 'sp'), may hold values from -0.15625 to 0.15625
Outputs:
- layer_out: bfloat16 [12288, 2048], P('sp', 'tp')
All inputs are finite; a program needn't handle non-finite values.
Results may differ from a plain program's by a relative error of at most 0.012.
The roundings to bfloat16 on the way count: a program that leaves them out, or rounds other values in their place, can miss the bound.
Values may be sent and summed in bfloat16 or wider, within the bound.
A program may use at most 64 MiB of HBM per device.

v0:
```python
import jax
import jax.numpy as jnp
from jax import lax
from jax.sharding import PartitionSpec as P

D = 2048
HEAD_SIZE = 128
QUERY_HEADS = 8
KEY_VALUE_HEADS = 2
GRID = 64


eps = 1e-06
rotary_base = 10000.0


def sent_together(arrays, axis, dim, along):
    ends, at = ([], 0)
    for a in arrays[:-1]:
        at += a.shape[along]
        ends.append(at)
    both = jnp.concatenate(arrays, axis=along)
    return tuple(jnp.split(lax.all_gather(both, axis, axis=dim, tiled=True), ends, axis=along))


def laid_out(tiles, dim):
    tiles = jnp.moveaxis(tiles, 0, dim)
    lengths = tiles.shape
    return tiles.reshape(*lengths[:dim], lengths[dim] * lengths[dim + 1], *lengths[dim + 2 :])


def sent_to_all(x, axis):
    size = lax.axis_size(axis)
    return lax.all_to_all(jnp.broadcast_to(x[None], (size, *x.shape)), axis, 0, 0, tiled=True)


def gathered_copies(x, axis, dim):
    return laid_out(sent_to_all(x, axis), dim)


def taken_together(x, axis):
    everything = sent_to_all(x, axis)
    return jnp.sum(everything, axis=0)


def in_blocks(x, dim, size):
    lengths = x.shape
    tiles = x.reshape(*lengths[:dim], size, lengths[dim] // size, *lengths[dim + 1 :])
    return jnp.moveaxis(tiles, dim, 0)


def summed_on_arrival(x, axis, dim):
    tiles = in_blocks(x, dim, lax.axis_size(axis))
    arrived = lax.all_to_all(tiles, axis, split_axis=0, concat_axis=0, tiled=True)
    return arrived.astype(jnp.float32).sum(axis=0)


def apply_rotary(vectors, grid_positions):
    half_size = vectors.shape[-1] // 2
    frequency = rotary_base ** (-jnp.arange(0, half_size, 2, dtype=jnp.float32) / half_size)
    grid_row = (grid_positions // GRID).astype(jnp.float32)
    grid_col = (grid_positions % GRID).astype(jnp.float32)
    angles = jnp.concatenate(
        [grid_row[:, None] * frequency, grid_col[:, None] * frequency], axis=-1
    )[:, None, :]
    cosine_table = jnp.cos(angles)
    sine_table = jnp.sin(angles)
    first_half = vectors[..., :half_size]
    second_half = vectors[..., half_size:]
    return jnp.concatenate(
        [
            first_half * cosine_table - second_half * sine_table,
            first_half * sine_table + second_half * cosine_table,
        ],
        axis=-1,
    )


def per_head_norm(vectors, gain):
    return vectors * lax.rsqrt(jnp.mean(vectors * vectors, axis=-1, keepdims=True) + eps) * gain


def on_device(
    residual_in,
    queries,
    keys,
    values,
    query_gain,
    key_norm_gain,
    out_weight,
    mlp_gain,
    gate_weight,
    up_weight,
    down_weight,
):
    local_rows = residual_in.shape[0]
    local_heads = queries.shape[1] // HEAD_SIZE
    queries_per_group = QUERY_HEADS // KEY_VALUE_HEADS
    tp_index = lax.axis_index("tp")
    tp_count = lax.axis_size("tp")
    grid_positions = lax.axis_index("sp") * local_rows + jnp.arange(local_rows, dtype=jnp.int32)
    weight_cols = lax.all_to_all(out_weight, "tp", split_axis=1, concat_axis=0, tiled=True)
    query_rows = apply_rotary(
        per_head_norm(
            queries.astype(jnp.float32).reshape(local_rows, local_heads, HEAD_SIZE), query_gain
        ),
        grid_positions,
    ).astype(jnp.bfloat16)
    query_matrix = jnp.transpose(query_rows, (1, 0, 2)).reshape(local_heads * local_rows, HEAD_SIZE)
    shared = tp_index * local_heads // queries_per_group
    own_keys = lax.dynamic_slice_in_dim(keys, shared * HEAD_SIZE, HEAD_SIZE, 1)
    own_values = lax.dynamic_slice_in_dim(values, shared * HEAD_SIZE, HEAD_SIZE, 1)
    key_matrix = apply_rotary(
        per_head_norm(own_keys.astype(jnp.float32)[:, None, :], key_norm_gain), grid_positions
    )[:, 0, :].astype(jnp.bfloat16)
    score_scale = HEAD_SIZE ** (-0.5)
    query_count = local_heads * local_rows
    start_state = (
        jnp.full((query_count,), -1e30, jnp.float32),
        jnp.zeros((query_count,), jnp.float32),
        jnp.zeros((query_count, HEAD_SIZE), jnp.float32),
    )
    key_piece, value_piece = sent_together((key_matrix, own_values), "sp", 0, 1)
    piece_rows = key_piece.shape[0]
    block_count = -(-piece_rows // 2048)
    while piece_rows % block_count:
        block_count += 1
    block_width = piece_rows // block_count

    def one_block(block_index, state_inner):
        running_max, running_sum, weighted = state_inner
        block_keys = lax.dynamic_slice_in_dim(key_piece, block_index * block_width, block_width, 0)
        block_values = lax.dynamic_slice_in_dim(
            value_piece, block_index * block_width, block_width, 0
        )
        scores = (
            jnp.dot(query_matrix, block_keys.T, preferred_element_type=jnp.float32) * score_scale
        )
        new_max = jnp.maximum(running_max, jnp.max(scores, axis=1))
        factor = jnp.exp(running_max - new_max)
        weights = jnp.exp(scores - new_max[:, None])
        running_sum = running_sum * factor + jnp.sum(weights, axis=1)
        weighted = weighted * factor[:, None] + jnp.dot(
            weights.astype(jnp.bfloat16), block_values, preferred_element_type=jnp.float32
        )
        return (new_max, running_sum, weighted)

    running_max, running_sum, weighted = lax.fori_loop(0, block_count, one_block, start_state)
    attended = (weighted / running_sum[:, None]).astype(jnp.bfloat16)
    attended = jnp.transpose(
        attended.reshape(local_heads, local_rows, HEAD_SIZE), (1, 0, 2)
    ).reshape(local_rows, local_heads * HEAD_SIZE)
    own_width = residual_in.shape[1]
    attended_full = gathered_copies(attended, "tp", 1)
    group_width = local_heads * HEAD_SIZE
    share = jnp.zeros((local_rows, own_width), jnp.float32)
    for group_index in range(tp_count):
        left_part = attended_full[:, group_index * group_width : (group_index + 1) * group_width]
        right_part = weight_cols[group_index * group_width : (group_index + 1) * group_width, :]
        term = jnp.dot(left_part, right_part, preferred_element_type=jnp.float32).astype(
            jnp.bfloat16
        )
        share = share + term.astype(jnp.float32)
    residual_mid = residual_in.astype(jnp.float32) + share
    squares = taken_together(jnp.sum(residual_mid * residual_mid, axis=1), "tp")
    gain_own = lax.dynamic_slice_in_dim(mlp_gain, tp_index * own_width, own_width, 0)
    normed_own = (residual_mid * lax.rsqrt(squares / D + eps)[:, None] * gain_own).astype(
        jnp.bfloat16
    )
    normed = lax.all_gather(normed_own, "tp", axis=1, tiled=True)
    pieces = sent_together((gate_weight, up_weight), "sp", 0, 1)
    gate_out = jnp.dot(normed, pieces[0], preferred_element_type=jnp.float32)
    up_out = jnp.dot(normed, pieces[1], preferred_element_type=jnp.float32)
    hidden = (jax.nn.silu(gate_out) * up_out).astype(jnp.bfloat16)
    down_terms = jnp.dot(
        hidden,
        lax.all_gather(down_weight, "sp", axis=1, tiled=True),
        preferred_element_type=jnp.float32,
    )
    down_share = summed_on_arrival(down_terms.astype(jnp.bfloat16), "tp", 1)
    return (residual_mid + 0.5 * down_share).astype(jnp.bfloat16)


def solution(mesh):
    in_specs = (
        P("sp", "tp"),
        P("sp", "tp"),
        P("sp", None),
        P("sp", None),
        P(),
        P(),
        P("tp", None),
        P(),
        P("sp", "tp"),
        P("sp", "tp"),
        P("tp", "sp"),
    )
    out_specs = P("sp", "tp")
    return jax.shard_map(
        on_device, mesh=mesh, in_specs=in_specs, out_specs=out_specs, check_vma=False
    )
```

profile of v0, /device:TPU:1, one launch (start us, length us, event | category | flops | bytes accessed | tf_op | source)
XLA Modules:
  0.0 336.8 jit_solution(7837900333065985362)
XLA Ops:
  6.6 1.1 fusion.38
  7.7 1.1 fusion.41
  8.9 0.3 multiply_bitcast_fusion.1
  9.2 1.3 fusion.40
  10.5 1.8 fusion.44
  12.3 0.3 subtract_convert_fusion.1
  12.8 0.8 pad_maximum_fusion.1
  13.6 1.0 copy.61
  14.6 5.8 %all-to-all-start.1 = ((bf16[128,8,256]{0,2,1:T(8,128)(2,1)}), bf16[128,8,256]{0,2,1:T(8,128)(2,1)S(1)}, u32[]{:S(2)}, u32[]{:S(2)}) async-start(bf16[128,8,256]{0,2,1:T(8,128)(2,1)} %bitcast.9), calls=%async_computation.1 | async-start | bytes 1048576 | tf_op jit(solution)/shard_map/all_to_all | solution.py:102
  20.4 0.8 pad_maximum_fusion.2
  21.4 56.8 %all-gather.5.cloned.1.call-done = bf16[12288,256]{1,0:T(8,128)(2,1)} async-done(((bf16[768,256]{1,0:T(8,128)(2,1)}), bf16[12288,256]{1,0:T(8,128)(2,1)}) %all-gather.5.cloned.1.call-update) | async-done | bytes 6291472 | tf_op jit(solution)/shard_map/all_gather | solution.py:23
  78.2 4.7 %fusion.66 = (bf16[12288,128]{1,0:T(8,128)(2,1)}, bf16[12288,128]{1,0:T(8,128)(2,1)}) fusion(bf16[12288,256]{1,0:T(8,128)(2,1)} %all-gather.5.cloned.1.call-done), kind=kLoop, calls=%fused_computation.114 | loop fusion | bytes 12582912 | tf_op jit(solution)/shard_map/split | solution.py:23
  82.9 71.6 %while.18 = (s32[]{:T(128)}, f32[768]{0:T(1024)S(1)}, f32[768]{0:T(1024)S(1)}, f32[768,128]{1,0:T(8,128)S(1)}, bf16[12288,128]{1,0:T(8,128)(2,1)}, /*index=5*/bf...) while((s32[]{:T(128)}, f32[768]{0:T(1024)S(1)}, ...), condition=%wide.region_5.6_spmd.clone, body=%wide.region_2.5_spmd.clone.sunk | while | flops 818188032 | bytes 46121160 | solution.py:148
  82.9 4.7 %multiply_reduce_fusion.3 = (f32[768]{0:T(1024)S(1)}, f32[2048,768]{1,0:T(8,128)}) fusion(bf16[768,128]{1,0:T(8,128)(2,1)S(1)} %get-tuple-element.268, bf16[12288,128]{1,0:T(8,128)(2,1)} %get-tuple-element.267, s32[]{:T(128)S(6)} %select_n.55), kind=kOutput, calls=%fused_computation.1.clone.1 | convolution fusion | flops 405798144 | bytes 7015428 | tf_op jit(solution)/shard_map/while/body/eval_jaxpr/dot_general | solution.py:137
  87.6 4.2 %fusion.80 = f32[768]{0:T(1024)S(1)} fusion(f32[2048,768]{1,0:T(8,128)} %get-tuple-element.238, f32[768]{0:T(1024)S(1)} %select_maximum_fusion.2), kind=kLoop, calls=%fused_computation.3.clone.1 | loop fusion | flops 4717824 | bytes 6297600 | tf_op jit(solution)/shard_map/while/body/eval_jaxpr/reduce_sum | solution.py:142
  91.8 0.8 copy-done.1
  92.6 2.4 fusion.82
  95.0 4.7 %multiply_reduce_fusion.3 = (f32[768]{0:T(1024)S(1)}, f32[2048,768]{1,0:T(8,128)}) fusion(bf16[768,128]{1,0:T(8,128)(2,1)S(1)} %get-tuple-element.268, bf16[12288,128]{1,0:T(8,128)(2,1)} %get-tuple-element.267, s32[]{:T(128)S(6)} %select_n.55), kind=kOutput, calls=%fused_computation.1.clone.1 | convolution fusion | flops 405798144 | bytes 7015428 | tf_op jit(solution)/shard_map/while/body/eval_jaxpr/dot_general | solution.py:137
  99.6 4.1 %fusion.80 = f32[768]{0:T(1024)S(1)} fusion(f32[2048,768]{1,0:T(8,128)} %get-tuple-element.238, f32[768]{0:T(1024)S(1)} %select_maximum_fusion.2), kind=kLoop, calls=%fused_computation.3.clone.1 | loop fusion | flops 4717824 | bytes 6297600 | tf_op jit(solution)/shard_map/while/body/eval_jaxpr/reduce_sum | solution.py:142
  103.7 0.6 copy-done.1
  104.3 2.4 fusion.82
  106.7 4.7 %multiply_reduce_fusion.3 = (f32[768]{0:T(1024)S(1)}, f32[2048,768]{1,0:T(8,128)}) fusion(bf16[768,128]{1,0:T(8,128)(2,1)S(1)} %get-tuple-element.268, bf16[12288,128]{1,0:T(8,128)(2,1)} %get-tuple-element.267, s32[]{:T(128)S(6)} %select_n.55), kind=kOutput, calls=%fused_computation.1.clone.1 | convolution fusion | flops 405798144 | bytes 7015428 | tf_op jit(solution)/shard_map/while/body/eval_jaxpr/dot_general | solution.py:137
  111.4 4.2 %fusion.80 = f32[768]{0:T(1024)S(1)} fusion(f32[2048,768]{1,0:T(8,128)} %get-tuple-element.238, f32[768]{0:T(1024)S(1)} %select_maximum_fusion.2), kind=kLoop, calls=%fused_computation.3.clone.1 | loop fusion | flops 4717824 | bytes 6297600 | tf_op jit(solution)/shard_map/while/body/eval_jaxpr/reduce_sum | solution.py:142
  115.6 0.8 copy-done.1
  116.4 2.4 fusion.82
  118.8 4.7 %multiply_reduce_fusion.3 = (f32[768]{0:T(1024)S(1)}, f32[2048,768]{1,0:T(8,128)}) fusion(bf16[768,128]{1,0:T(8,128)(2,1)S(1)} %get-tuple-element.268, bf16[12288,128]{1,0:T(8,128)(2,1)} %get-tuple-element.267, s32[]{:T(128)S(6)} %select_n.55), kind=kOutput, calls=%fused_computation.1.clone.1 | convolution fusion | flops 405798144 | bytes 7015428 | tf_op jit(solution)/shard_map/while/body/eval_jaxpr/dot_general | solution.py:137
  123.5 4.2 %fusion.80 = f32[768]{0:T(1024)S(1)} fusion(f32[2048,768]{1,0:T(8,128)} %get-tuple-element.238, f32[768]{0:T(1024)S(1)} %select_maximum_fusion.2), kind=kLoop, calls=%fused_computation.3.clone.1 | loop fusion | flops 4717824 | bytes 6297600 | tf_op jit(solution)/shard_map/while/body/eval_jaxpr/reduce_sum | solution.py:142
  127.7 0.8 copy-done.1
  128.5 2.4 fusion.82
  130.9 4.7 %multiply_reduce_fusion.3 = (f32[768]{0:T(1024)S(1)}, f32[2048,768]{1,0:T(8,128)}) fusion(bf16[768,128]{1,0:T(8,128)(2,1)S(1)} %get-tuple-element.268, bf16[12288,128]{1,0:T(8,128)(2,1)} %get-tuple-element.267, s32[]{:T(128)S(6)} %select_n.55), kind=kOutput, calls=%fused_computation.1.clone.1 | convolution fusion | flops 405798144 | bytes 7015428 | tf_op jit(solution)/shard_map/while/body/eval_jaxpr/dot_general | solution.py:137
  135.6 4.2 %fusion.80 = f32[768]{0:T(1024)S(1)} fusion(f32[2048,768]{1,0:T(8,128)} %get-tuple-element.238, f32[768]{0:T(1024)S(1)} %select_maximum_fusion.2), kind=kLoop, calls=%fused_computation.3.clone.1 | loop fusion | flops 4717824 | bytes 6297600 | tf_op jit(solution)/shard_map/while/body/eval_jaxpr/reduce_sum | solution.py:142
  139.8 0.7 copy-done.1
  140.5 2.4 fusion.82
  142.9 4.7 %multiply_reduce_fusion.3 = (f32[768]{0:T(1024)S(1)}, f32[2048,768]{1,0:T(8,128)}) fusion(bf16[768,128]{1,0:T(8,128)(2,1)S(1)} %get-tuple-element.268, bf16[12288,128]{1,0:T(8,128)(2,1)} %get-tuple-element.267, s32[]{:T(128)S(6)} %select_n.55), kind=kOutput, calls=%fused_computation.1.clone.1 | convolution fusion | flops 405798144 | bytes 7015428 | tf_op jit(solution)/shard_map/while/body/eval_jaxpr/dot_general | solution.py:137
  147.5 4.0 %fusion.80 = f32[768]{0:T(1024)S(1)} fusion(f32[2048,768]{1,0:T(8,128)} %get-tuple-element.238, f32[768]{0:T(1024)S(1)} %select_maximum_fusion.2), kind=kLoop, calls=%fused_computation.3.clone.1 | loop fusion | flops 4717824 | bytes 6297600 | tf_op jit(solution)/shard_map/while/body/eval_jaxpr/reduce_sum | solution.py:142
  151.6 0.6 copy-done.1
  152.1 2.4 fusion.82
  154.9 1.3 broadcast_in_dim.17
  156.2 5.2 %all-to-all-start = ((bf16[8,768,128]{1,2,0:T(8,128)(2,1)}), bf16[8,768,128]{1,2,0:T(8,128)(2,1)S(1)}, u32[]{:S(2)}, u32[]{:S(2)}) async-start(bf16[8,768,128]{1,2,0:T(8,128)(2,1)} %broadcast_in_dim.17), calls=%async_computation | async-start | bytes 3145728 | tf_op jit(solution)/shard_map/all_to_all | solution.py:34
  161.4 1.9 copy.59
  163.3 18.7 %all-to-all-done = bf16[8,768,128]{1,2,0:T(8,128)(2,1)S(1)} async-done(((bf16[8,768,128]{1,2,0:T(8,128)(2,1)}), bf16[8,768,128]{1,2,0:T(8,128)(2,1)S(1)}, u32[]{:S(2)}, u32[]{:S(2)}) %all-to-all-start) | async-done | bytes 1572896 | tf_op jit(solution)/shard_map/all_to_all | solution.py:34
  182.0 0.2 fusion.35
  182.2 0.2 fusion.34
  182.5 0.2 fusion.32
  182.7 0.2 fusion.30
  183.0 0.2 fusion.28
  183.2 0.2 fusion.26
  183.5 0.2 fusion.24
  184.0 0.3 multiply_reduce_fusion.1
  184.3 0.6 broadcast_in_dim.18
  184.9 4.2 %all-to-all-start.2 = ((f32[8,1,768]{2,1,0:T(1,128)}), f32[8,1,768]{2,1,0:T(1,128)S(1)}, u32[]{:S(2)}, u32[]{:S(2)}) async-start(f32[8,1,768]{2,1,0:T(1,128)} %broadcast_in_dim.18), calls=%async_computation.2 | async-start | bytes 49152 | tf_op jit(solution)/shard_map/all_to_all | solution.py:34
  189.1 0.8 dynamic_slice.25
  189.9 3.9 %all-to-all-done.2 = f32[8,1,768]{2,1,0:T(1,128)S(1)} async-done(((f32[8,1,768]{2,1,0:T(1,128)}), f32[8,1,768]{2,1,0:T(1,128)S(1)}, u32[]{:S(2)}, u32[]{:S(2)}) %all-to-all-start.2) | async-done | bytes 24608 | tf_op jit(solution)/shard_map/all_to_all | solution.py:34
  193.9 0.9 multiply_convert_fusion.1
  195.0 0.3 all-gather.11.cloned.1.call-update
  195.3 24.9 %all-gather.7.cloned.1.call-done = bf16[768,2048]{0,1:T(8,128)(2,1)} async-done(((bf16[768,256]{0,1:T(8,128)(2,1)}), bf16[768,2048]{0,1:T(8,128)(2,1)}) %all-gather.7.cloned.1.call-update) | async-done | bytes 3145744 | tf_op jit(solution)/shard_map/all_gather | solution.py:170
  220.2 5.2 %fusion.16 = f32[768,704]{0,1:T(8,128)S(1)} fusion(bf16[768,2048]{0,1:T(8,128)(2,1)} %all-gather.7.cloned.1.call-done, bf16[2048,1408]{0,1:T(8,128)(2,1)} %all-gather.9.cloned.1.call-done), kind=kOutput, calls=%fused_computation.22 | convolution fusion | flops 2214592512 | bytes 8192000 | tf_op jit(solution)/shard_map/dot_general | solution.py:172
  225.4 45.8 %all-gather.11.cloned.1.call-done = bf16[704,2048]{1,0:T(8,128)(2,1)} async-done(((bf16[704,128]{1,0:T(8,128)(2,1)}), bf16[704,2048]{1,0:T(8,128)(2,1)}) %all-gather.11.cloned.1.call-update) | async-done | bytes 2883600 | tf_op jit(solution)/shard_map/all_gather | solution.py:177
  271.2 11.7 %convolution_convert_fusion = bf16[768,2048]{1,0:T(8,128)(2,1)} fusion(bf16[704,2048]{1,0:T(8,128)(2,1)} %all-gather.11.cloned.1.call-done, f32[768,704]{0,1:T(8,128)S(1)} %fusion.16, bf16[768,2048]{0,1:T(8,128)(2,1)} %all-gather.7.cloned.1.call-done, bf16[2048,1408]{0,1:T(8,128)(2,1)} %all-gather.9.cloned.1.call-done), kind=kOutput, calls=%fused_computation.18 | convolution fusion | flops 4434001920 | bytes 14221312 | tf_op jit(solution)/shard_map/dot_general | solution.py:175
  282.9 2.1 copy.79
  285.0 43.5 %all_to_all.32 = bf16[8,768,256]{2,1,0:T(8,128)(2,1)S(1)} all-to-all(bf16[8,768,256]{2,1,0:T(8,128)(2,1)S(1)} %bitcast.66), channel_id=1, replica_groups=mesh['sp'=16,'tp'=8] {'tp'}, dimensions={0} | all-to-all | bytes 6291456 | tf_op jit(solution)/shard_map/all_to_all | solution.py:54
  328.5 0.4 convert_reduce_fusion
  329.0 0.3 copy.73
  329.3 0.9 copy.74
  (58 shorter events, 1.4 us)
Async XLA Ops:
  6.5 2.4 copy-start
  6.5 71.7 %all-gather.5.cloned.1.call-start = ((), (), s32[]{:S(2)}) async-start(), calls=%async_computation.4 | async-start | bytes 6684672 | tf_op jit(solution)/shard_map/all_gather | solution.py:23
  10.5 3.1 copy-start.3
  12.3 8.1 %copy-start.4 = (bf16[128,704]{0,1:T(8,128)(2,1)S(1)}, bf16[128,704]{0,1:T(8,128)(2,1)}, u32[]{:S(2)}) copy-start(bf16[128,704]{0,1:T(8,128)(2,1)} %param.22) | copy-start | bytes 540676
  12.3 8.1 %copy-start.5 = (bf16[128,704]{0,1:T(8,128)(2,1)S(1)}, bf16[128,704]{0,1:T(8,128)(2,1)}, u32[]{:S(2)}) copy-start(bf16[128,704]{0,1:T(8,128)(2,1)} %param.21) | copy-start | bytes 540676
  14.6 140.2 %all-to-all-start.1 = ((bf16[128,8,256]{0,2,1:T(8,128)(2,1)}), bf16[128,8,256]{0,2,1:T(8,128)(2,1)S(1)}, u32[]{:S(2)}, u32[]{:S(2)}) async-start(bf16[128,8,256]{0,2,1:T(8,128)(2,1)} %bitcast.9), calls=%async_computation.1 | async-start | bytes 1048576 | tf_op jit(solution)/shard_map/all_to_all | solution.py:102
  20.4 174.9 %all-gather.9.cloned.1.call-start = ((), (), s32[]{:S(2)}) async-start(), calls=%async_computation.6 | async-start | bytes 6127616 | tf_op jit(solution)/shard_map/all_gather | solution.py:23
  87.6 5.0 %copy-start.1 = (f32[2048,768]{1,0:T(8,128)S(1)}, f32[2048,768]{1,0:T(8,128)}, u32[]{:S(2)}) copy-start(f32[2048,768]{1,0:T(8,128)} %get-tuple-element.238) | copy-start | bytes 18874372 | tf_op jit(solution)/shard_map/while
  99.6 4.7 %copy-start.1 = (f32[2048,768]{1,0:T(8,128)S(1)}, f32[2048,768]{1,0:T(8,128)}, u32[]{:S(2)}) copy-start(f32[2048,768]{1,0:T(8,128)} %get-tuple-element.238) | copy-start | bytes 18874372 | tf_op jit(solution)/shard_map/while
  111.4 5.0 %copy-start.1 = (f32[2048,768]{1,0:T(8,128)S(1)}, f32[2048,768]{1,0:T(8,128)}, u32[]{:S(2)}) copy-start(f32[2048,768]{1,0:T(8,128)} %get-tuple-element.238) | copy-start | bytes 18874372 | tf_op jit(solution)/shard_map/while
  123.5 5.0 %copy-start.1 = (f32[2048,768]{1,0:T(8,128)S(1)}, f32[2048,768]{1,0:T(8,128)}, u32[]{:S(2)}) copy-start(f32[2048,768]{1,0:T(8,128)} %get-tuple-element.238) | copy-start | bytes 18874372 | tf_op jit(solution)/shard_map/while
  135.6 4.9 %copy-start.1 = (f32[2048,768]{1,0:T(8,128)S(1)}, f32[2048,768]{1,0:T(8,128)}, u32[]{:S(2)}) copy-start(f32[2048,768]{1,0:T(8,128)} %get-tuple-element.238) | copy-start | bytes 18874372 | tf_op jit(solution)/shard_map/while
  147.5 4.6 %copy-start.1 = (f32[2048,768]{1,0:T(8,128)S(1)}, f32[2048,768]{1,0:T(8,128)}, u32[]{:S(2)}) copy-start(f32[2048,768]{1,0:T(8,128)} %get-tuple-element.238) | copy-start | bytes 18874372 | tf_op jit(solution)/shard_map/while
  156.2 25.8 %all-to-all-start = ((bf16[8,768,128]{1,2,0:T(8,128)(2,1)}), bf16[8,768,128]{1,2,0:T(8,128)(2,1)S(1)}, u32[]{:S(2)}, u32[]{:S(2)}) async-start(bf16[8,768,128]{1,2,0:T(8,128)(2,1)} %broadcast_in_dim.17), calls=%async_computation | async-start | bytes 3145728 | tf_op jit(solution)/shard_map/all_to_all | solution.py:34
  183.0 1.0 copy-start.2
  184.9 8.9 %all-to-all-start.2 = ((f32[8,1,768]{2,1,0:T(1,128)}), f32[8,1,768]{2,1,0:T(1,128)S(1)}, u32[]{:S(2)}, u32[]{:S(2)}) async-start(f32[8,1,768]{2,1,0:T(1,128)} %broadcast_in_dim.18), calls=%async_computation.2 | async-start | bytes 49152 | tf_op jit(solution)/shard_map/all_to_all | solution.py:34
  189.1 31.1 %all-gather.7.cloned.1.call-start = ((), (), s32[]{:S(2)}) async-start(), calls=%async_computation.5 | async-start | bytes 3538944 | tf_op jit(solution)/shard_map/all_gather | solution.py:170
  194.7 76.4 %all-gather.11.cloned.1.call-start = ((), (), s32[]{:S(2)}) async-start(), calls=%async_computation.7 | async-start | bytes 3063808 | tf_op jit(solution)/shard_map/all_gather | solution.py:177
Sparse Core Ops, SparseCore 0:
  13.7 64.4 all-gather.4
  80.3 62.8 all-gather.8
  194.9 25.3 all-gather.6
  222.2 48.9 all-gather.10
where the time goes:
time: 338 us; the launch traced here: 337 us
  waiting for transfers between devices  151 us (45%)
  matrix products  61.1 us (18%)
  blocking collectives  43.5 us (13%)
  other arithmetic  34.3 us (10%)
  local copies, waits for them, and re-layouts  18.2 us (5%)
  starting transfers between devices  15.5 us (5%)
  between operations  13.4 us (4%)
    all_gather x2, waiting for transfers between devices, sent_together(): lax.all_gather(both, axis, axis=dim, tiled=True)  56.8 us
    all_gather x1, waiting for transfers between devices, on_device(): lax.all_gather(down_weight, 'sp', axis=1, tiled=True)  45.8 us
    all_to_all x1, blocking collectives, summed_on_arrival(): lax.all_to_all(tiles, axis, split_axis=0, concat_axis=0, tiled=True)  43.5 us
    dot_general x6, matrix products, one_block(): jnp.dot(query_matrix, block_keys.T, preferred_element_type=jnp.float32)  28 us
    all_gather x1, waiting for transfers between devices, on_device(): normed = lax.all_gather(normed_own, 'tp', axis=1, tiled=True)  24.9 us
    reduce_sum x6, other arithmetic, one_block(): running_sum = running_sum * factor + jnp.sum(weights, axis=1)  24.8 us
    all_to_all x2, waiting for transfers between devices, sent_to_all(): lax.all_to_all(jnp.broadcast_to(x[None], (size, *x.shape)), axis, 0, 0, t...  22.6 us
    dot_general x6, matrix products, one_block(): jnp.dot(weights.astype(jnp.bfloat16), block_values, preferred_element_typ...  14.2 us
  transfers between devices with their start and end apart: 7, of which 5 were waited for; matrix products, arithmetic and copies ran while one was open for 26% of the time, Pallas kernels for 0%

commit v1 on v0

v1 whole, which is shorter than its diff:
```python
import functools
import math

import jax
import jax.numpy as jnp
import numpy as np
from jax import lax
from jax.experimental import pallas as pl
from jax.experimental.pallas import tpu as pltpu
from jax.sharding import PartitionSpec as P

D = 2048
HEAD = 128
GRID = 64
ROWS = 768
FF_DEV = 704
EPS = 1e-06
CHUNKS = 3
CT = ROWS // CHUNKS
XR = CT + 16
LOG2E = 1.4426950408889634
SCORE = HEAD ** (-0.5) * LOG2E
MESH = pl.DeviceIdType.MESH
F32 = jnp.float32
BF16 = jnp.bfloat16

ORDER = [(0, 0), (0, 3), (3, 0), (0, 1), (1, 0), (0, 2), (2, 0), (3, 3), (3, 1), (1, 3), (1, 1), (3, 2), (2, 3), (1, 2), (2, 1), (2, 2)]
LOOK = 2
GU_AT = 10


def rotary_tables():
    half = HEAD // 2
    freq = (10000.0 ** (-np.arange(0, half, 2, dtype=np.float32) / np.float32(half))).astype(np.float32)
    lanes = np.arange(HEAD)
    of_row = (lanes % 64) < 32
    sign = np.where(lanes < 64, -1.0, 1.0)
    f = freq[lanes % 32]
    out = []
    for count, mask in ((12288 // GRID, of_row), (GRID, ~of_row)):
        ang = (np.arange(count, dtype=np.float32)[:, None] * f[None, :]).astype(np.float32).astype(np.float64)
        out.append(np.where(mask, np.cos(ang), 0.0).astype(np.float32))
        out.append(np.where(mask, np.sin(ang) * sign, 0.0).astype(np.float32))
    return out


def kernel(
    res_ref, q_ref, k_ref, v_ref, qg_ref, kg_ref, wo_ref, mg_ref, g_ref, u_ref, dw_ref,
    rc_ref, rs_ref, cc_ref, cs_ref,
    out_ref,
    kv, gu, dn, att, wo, xn, hid, tb, ob, rb, sb, pb, fb, rm, qT, m_s, acc,
    kv_ss, kv_rs, w_ss, w_rs, rel_ss, rel_rs, wo_ss, wo_rs, at_ss, at_rs, ad_ss, ad_rs,
    xs_ss, xs_rs, xd_ss, xd_rs, td_ss, td_rs, p_ss, p_rs, f_ss, f_rs,
):
    sp = lax.axis_index("sp")
    tp = lax.axis_index("tp")
    z, y = sp // 4, sp % 4
    x, core = tp // 2, tp % 2

    def bid(a, b):
        return ((z + a) % 4) * 4 + (y + b) % 4

    def near(dz, dy):
        return {"sp": bid(dz, dy), "tp": tp}

    def xdev(dx):
        return {"sp": sp, "tp": ((x + dx) % 4) * 2 + core}

    partner_tp = x * 2 + 1 - core
    partner = {"sp": sp, "tp": partner_tp}

    def copy(src, dst, ss, rs, dev):
        return pltpu.make_async_remote_copy(src_ref=src, dst_ref=dst, send_sem=ss, recv_sem=rs, device_id=dev, device_id_type=MESH)

    def when(cond, fn):
        if isinstance(cond, (bool, np.bool_)):
            if cond:
                fn()
        else:
            pl.when(cond)(fn)

    barrier = pltpu.get_barrier_semaphore()
    peers = [near(0, 1), near(0, 3), near(1, 0), near(3, 0)]
    peers += [{"sp": sp, "tp": (tp + d) % 8} for d in range(1, 8)]
    for dev in peers:
        pl.semaphore_signal(barrier, inc=1, device_id=dev, device_id_type=MESH)

    def rotated(ref, lane0, gain, g):
        t = ref[g * 64 : (g + 1) * 64, pl.ds(lane0, HEAD)].astype(F32)
        t = t * lax.rsqrt(jnp.mean(t * t, axis=1, keepdims=True) + EPS) * gain
        grid_row = sp * (ROWS // GRID) + g
        cos = rc_ref[pl.ds(grid_row, 1), :] + cc_ref[...]
        sin = rs_ref[pl.ds(grid_row, 1), :] + cs_ref[...]
        return t * cos + pltpu.roll(t, 64, 1) * sin

    lane0 = pl.multiple_of((tp // 4) * HEAD, HEAD)
    kgain = kg_ref[...]
    qgain = qg_ref[...]
    for g in range(ROWS // GRID):
        kv[0, sp, g // 2, pl.ds((g % 2) * 64, 64), :] = rotated(k_ref, lane0, kgain, g).astype(BF16)
    for i in range(6):
        vi = v_ref[i * 128 : (i + 1) * 128, pl.ds(lane0, HEAD)].astype(F32)
        kv[1, sp, i] = vi.T.astype(BF16)

    pl.semaphore_wait(barrier, len(peers))

    def gather(piece, ss, rs, first):
        def send(a, b, dz, dy):
            at = ((a - dz + 4) % 4) * 4 + (b - dy + 4) % 4
            ref = piece(bid(a, b))
            copy(ref, ref, ss, rs.at[at], near(dz, dy)).start()

        def step(a, b, own=False):
            u, w = (b, a) if first == "y" else (a, b)
            if not own:
                ref = piece(bid(a, b))
                copy(ref, ref, ss, rs.at[a * 4 + b], near(0, 1)).wait_recv()

            def go(du, dw):
                dz, dy = (dw, du) if first == "y" else (du, dw)
                return lambda: send(a, b, dz, dy)

            if own:
                for du, dw in ((1, 0), (3, 0), (0, 1), (0, 3)):
                    go(du, dw)()
            else:
                even = u % 2 == 0
                if isinstance(u, int):
                    when(w == 0 and u == 3, go(1, 0))
                    when(w == 0 or (w == 3 and even), go(0, 1))
                    when(w == 0 or (w == 1 and not even), go(0, 3))
                else:
                    when((w == 0) & (u == 3), go(1, 0))
                    when((w == 0) | ((w == 3) & even), go(0, 1))
                    when((w == 0) | ((w == 1) & (u % 2 == 1)), go(0, 3))

        def drain():
            ref = piece(pl.ds(0, 15))
            copy(ref, ref, ss, rs.at[0], near(0, 1)).wait_send()

        return step, drain

    kv_a = gather(lambda i: kv.at[core, i, 0:3], kv_ss.at[0], kv_rs.at[0], "y")
    kv_b = gather(lambda i: kv.at[core, i, 3:6], kv_ss.at[1], kv_rs.at[1], "z")
    gu_a = gather(lambda i: gu.at[i, 0:64], w_ss.at[0], w_rs.at[0], "y")
    gu_b = gather(lambda i: gu.at[i, 64:128], w_ss.at[1], w_rs.at[1], "z")
    dn_a = gather(lambda i: dn.at[i, 0:352], w_ss.at[2], w_rs.at[2], "y")
    dn_b = gather(lambda i: dn.at[i, 352:704], w_ss.at[3], w_rs.at[3], "z")

    def kv_step(a, b):
        kv_a[0](a, b)
        kv_b[0](a, b)
        ref = kv.at[core, bid(a, b)]
        copy(ref, ref, rel_ss, rel_rs.at[a * 4 + b], partner).start()

    def kv_relayed(a, b):
        ref = kv.at[1 - core, bid(a, b)]
        copy(ref, ref, rel_ss, rel_rs.at[a * 4 + b], partner).wait_recv()

    def gu_step(a, b, own=False):
        gu_a[0](a, b, own)
        gu_b[0](a, b, own)

    def dn_step(a, b, own=False):
        dn_a[0](a, b, own)
        dn_b[0](a, b, own)

    kv_a[0](0, 0, True)
    kv_b[0](0, 0, True)

    for d in range(1, 8):
        to = (tp + d) % 8
        copy(
            wo_ref.at[:, pl.ds(pl.multiple_of(to * 256, 256), 256)], wo.at[tp], wo_ss, wo_rs.at[8 - d], {"sp": sp, "tp": to}
        ).start()

    for g in range(ROWS // GRID):
        qT[:, g * 64 : (g + 1) * 64] = rotated(q_ref, 0, qgain, g).T.astype(BF16)
    m_s[...] = jnp.full_like(m_s, -1e30)
    acc[...] = jnp.zeros_like(acc)

    for n in range(5):
        gu[sp, :, n * 256 : n * 256 + 128] = g_ref[:, n * 128 : (n + 1) * 128]
        gu[sp, :, n * 256 + 128 : (n + 1) * 256] = u_ref[:, n * 128 : (n + 1) * 128]
    gu[sp, :, 1280:1408] = jnp.concatenate([g_ref[:, 640:704], u_ref[:, 640:704]], axis=1)
    dn[sp, 0:704, :] = dw_ref[...]
    for i in range(16):
        dn[i, 704:768, :] = jnp.zeros((64, 128), BF16)
    wo[tp] = wo_ref[:, pl.ds(pl.multiple_of(tp * 256, 256), 256)]

    def attend(blk):
        k = kv[0, blk].reshape(ROWS, HEAD)
        s = jnp.dot(k, qT[...], preferred_element_type=F32)
        old = m_s[...]
        new = jnp.maximum(old, jnp.max(s, axis=0, keepdims=True))
        factor = jnp.exp2((old - new) * SCORE)
        m_s[...] = new
        p = jnp.exp2((s - new) * SCORE).astype(BF16)
        v = kv[1, blk]
        vt = jnp.concatenate([v[i] for i in range(6)], axis=1)
        vt = jnp.concatenate([vt, jnp.ones((16, ROWS), BF16)], axis=0)
        acc[...] = acc[...] * factor + jnp.dot(vt, p, preferred_element_type=F32)

    def place(s):
        a, b = jnp.int32(0), jnp.int32(0)
        for i, (ai, bi) in enumerate(ORDER):
            a = jnp.where(s == i, ai, a)
            b = jnp.where(s == i, bi, b)
        return a, b

    attend(sp)
    for i in range(1, 1 + LOOK):
        kv_step(*ORDER[i])

    def att_loop(s, c):
        @pl.when(s + LOOK < 16)
        def _():
            kv_step(*place(s + LOOK))

        @pl.when(s == GU_AT)
        def _():
            gu_step(0, 0, True)

        @pl.when(s > GU_AT)
        def _():
            gu_step(*place(s - GU_AT))

        a, b = place(s)
        kv_relayed(a, b)
        attend(bid(a, b))
        return c

    lax.fori_loop(1, 16, att_loop, 0)

    todo = [functools.partial(gu_step, *ORDER[i]) for i in range(16 - GU_AT, 11)]
    todo += [functools.partial(dn_step, 0, 0, True)]
    todo += [functools.partial(gu_step, *ORDER[i]) for i in range(11, 16)]
    gu_left = len(todo)
    todo += [functools.partial(dn_step, *ORDER[i]) for i in range(1, 16)]
    done = [0]

    def pump(upto):
        while done[0] < upto:
            todo[done[0]]()
            done[0] += 1

    attn = (acc[0:HEAD, :] / acc[HEAD : HEAD + 1, :]).T.astype(BF16)
    att[tp] = attn

    def xgather(block, pieces, ss, rs, dss, drs):
        def own(dx):
            return ((x + dx) % 4) * 2 + core

        def send(dx, p, to):
            ref = block(own(dx), pieces[p])
            copy(ref, ref, ss.at[p], rs.at[((dx - to) % 4) * 2 + p], xdev(to)).start()

        def wait(dx, p):
            ref = block(own(dx), pieces[p])
            copy(ref, ref, ss.at[p], rs.at[(dx % 4) * 2 + p], xdev(1)).wait_recv()

        whole = (0, pieces[1][1])

        def relay(dx):
            ref = block(own(dx), whole)
            copy(ref, ref, dss, drs.at[dx % 4], partner).start()

        def start():
            send(0, 0, 1)
            send(0, 1, 3)
            send(0, 1, 1)
            send(0, 0, 3)
            relay(0)

        def forward():
            wait(3, 0)
            send(3, 0, 1)
            wait(1, 1)
            send(1, 1, 3)

        def finish():
            wait(3, 1)
            relay(3)
            wait(1, 0)
            relay(1)
            wait(2, 0)
            wait(2, 1)
            relay(2)

        def relayed():
            for dx in (0, 3, 1, 2):
                ref = block(((x + dx) % 4) * 2 + 1 - core, whole)
                copy(ref, ref, dss, drs.at[dx], partner).wait_recv()

        def drain():
            for p in range(2):
                ref = block(pl.ds(0, 3), pieces[p])
                copy(ref, ref, ss.at[p], rs.at[0], xdev(1)).wait_send()
            ref = block(pl.ds(0, 4), whole)
            copy(ref, ref, dss, drs.at[0], partner).wait_send()

        return start, forward, finish, relayed, drain

    def rows_of(ref):
        return lambda i, r: ref.at[i, r[0] : r[1]]

    at_x = xgather(rows_of(att), ((0, 384), (384, 768)), at_ss, at_rs, ad_ss, ad_rs)
    xn_x = [
        xgather(rows_of(xn.at[t]), ((0, 128), (128, XR)), xs_ss.at[t], xs_rs.at[t], xd_ss.at[t], xd_rs.at[t])
        for t in range(CHUNKS)
    ]
    at_x[0]()
    pump(2)
    at_x[1]()
    for d in range(1, 8):
        frm = (tp + d) % 8
        copy(wo.at[frm], wo.at[frm], wo_ss, wo_rs.at[d], {"sp": sp, "tp": frm}).wait_recv()
    pump(4)
    at_x[2]()
    at_x[3]()

    mgain = mg_ref[:, pl.ds(pl.multiple_of(tp * 256, 256), 256)]

    def project(t):
        rows = slice(t * CT, (t + 1) * CT)
        left = jnp.concatenate([att[i, rows] for i in range(8)], axis=1)
        mid = res_ref[rows, :].astype(F32) + jnp.dot(left, wo[...].reshape(8 * HEAD, 256), preferred_element_type=F32)
        rm[rows, :] = mid
        xn[t, tp, 0:CT, :] = (mid * mgain).astype(BF16)
        sq = jnp.sum((mid * mid).T, axis=0, keepdims=True)
        hi = sq.astype(BF16).astype(F32)
        row = lax.broadcasted_iota(jnp.int32, (16, CT), 0)
        xn[t, tp, CT:XR, :] = jnp.where(row == 0, hi, jnp.where(row == 1, sq - hi, 0.0)).astype(BF16)

    for t in range(CHUNKS):
        project(t)
        xn_x[t][0]()

    def gate_up(t):
        total = jnp.zeros((16, CT), F32)
        for i in range(8):
            total = total + xn[t, i, CT:XR, :].astype(F32)
        total = total[0:1, :] + total[1:2, :]
        scale = lax.rsqrt(total / D + EPS)
        scale = jnp.broadcast_to(scale, (128, CT)).T
        left = jnp.concatenate([xn[t, i, 0:CT, :] for i in range(8)], axis=1)

        def tile(n, c):
            w = gu[:, :, pl.ds(pl.multiple_of(n * 256, 256), 256)].reshape(D, 256)
            o = jnp.dot(left, w, preferred_element_type=F32)
            gate, up = o[:, 0:128] * scale, o[:, 128:256] * scale
            hid[t, :, pl.ds(pl.multiple_of(n * 128, 128), 128)] = (gate / (1.0 + jnp.exp(-gate)) * up).astype(BF16)
            return c

        lax.fori_loop(0, 5, tile, 0)
        w = gu[:, :, 1280:1408].reshape(D, 128)
        o = jnp.dot(left, w, preferred_element_type=F32) * scale
        tail = o / (1.0 + jnp.exp(-o)) * pltpu.roll(o, 64, 1)
        lane = lax.broadcasted_iota(jnp.int32, (CT, 128), 1)
        hid[t, :, 640:768] = jnp.where(lane < 64, tail, 0.0).astype(BF16)

    def down(t):
        def term(dst, c_of):
            def tile(dx, c):
                j = ((x + dx) % 4) * 2 + c_of
                w = jnp.concatenate([dn[2 * j], dn[2 * j + 1]], axis=1)
                dst[t, dx] = jnp.dot(hid[t], w, preferred_element_type=F32).astype(BF16)
                return c

            lax.fori_loop(0, 4, tile, 0)

        term(tb, 1 - core)
        copy(tb.at[t], rb.at[t], td_ss.at[t], td_rs.at[t], partner).start()
        term(ob, core)

    def both(t, dx):
        return ob[t, dx].astype(F32) + rb[t, dx].astype(F32)

    def reduce_far(t):
        copy(tb.at[t], rb.at[t], td_ss.at[t], td_rs.at[t], partner).wait_recv()
        sb[t, 0] = both(t, 2).astype(BF16)
        copy(sb.at[t, 0, 0:128], pb.at[t, 0], p_ss.at[t, 0], p_rs.at[t, 0], xdev(1)).start()
        copy(sb.at[t, 0, 128:256], pb.at[t, 1], p_ss.at[t, 1], p_rs.at[t, 1], xdev(3)).start()

    def reduce_near(t):
        copy(sb.at[t, 0, 0:128], pb.at[t, 0], p_ss.at[t, 0], p_rs.at[t, 0], xdev(1)).wait_recv()
        s = both(t, 1)
        sb[t, 1, 0:128, :] = (s[0:128] + pb[t, 0].astype(F32)).astype(BF16)
        sb[t, 1, 128:256, :] = s[128:256].astype(BF16)
        copy(sb.at[t, 1], fb.at[t, 0], f_ss.at[t, 0], f_rs.at[t, 0], xdev(1)).start()
        copy(sb.at[t, 0, 128:256], pb.at[t, 1], p_ss.at[t, 1], p_rs.at[t, 1], xdev(3)).wait_recv()
        s = both(t, 3)
        sb[t, 2, 0:128, :] = s[0:128].astype(BF16)
        sb[t, 2, 128:256, :] = (s[128:256] + pb[t, 1].astype(F32)).astype(BF16)
        copy(sb.at[t, 2], fb.at[t, 1], f_ss.at[t, 1], f_rs.at[t, 1], xdev(3)).start()

    def final(t):
        for i, dx in ((0, 1), (1, 3)):
            copy(sb.at[t, i + 1], fb.at[t, i], f_ss.at[t, i], f_rs.at[t, i], xdev(dx)).wait_recv()
        rows = slice(t * CT, (t + 1) * CT)
        total = both(t, 0) + fb[t, 0].astype(F32) + fb[t, 1].astype(F32)
        out_ref[rows, :] = (rm[rows, :] + 0.5 * total).astype(BF16)

    pump(gu_left - 3)
    xn_x[0][1]()
    pump(gu_left)
    xn_x[0][2]()
    xn_x[1][1]()
    xn_x[0][3]()
    gate_up(0)
    pump(gu_left + 5)
    xn_x[1][2]()
    xn_x[2][1]()
    xn_x[1][3]()
    gate_up(1)
    pump(gu_left + 10)
    xn_x[2][2]()
    xn_x[2][3]()
    gate_up(2)
    pump(len(todo))
    down(0)
    reduce_far(0)
    down(1)
    reduce_near(0)
    reduce_far(1)
    down(2)
    reduce_near(1)
    reduce_far(2)
    final(0)
    reduce_near(2)
    final(1)
    final(2)

    for _, drain in (kv_a, kv_b, gu_a, gu_b, dn_a, dn_b):
        drain()
    ref = kv.at[0, 0:15]
    copy(ref, ref, rel_ss, rel_rs.at[0], partner).wait_send()
    copy(wo.at[0:7], wo.at[0:7], wo_ss, wo_rs.at[0], partner).wait_send()
    at_x[4]()
    for t in range(CHUNKS):
        xn_x[t][4]()
        copy(tb.at[t], rb.at[t], td_ss.at[t], td_rs.at[t], partner).wait_send()
        copy(sb.at[t, 0, 0:128], pb.at[t, 0], p_ss.at[t, 0], p_rs.at[t, 0], xdev(1)).wait_send()
        copy(sb.at[t, 0, 128:256], pb.at[t, 1], p_ss.at[t, 1], p_rs.at[t, 1], xdev(3)).wait_send()
        copy(sb.at[t, 1], fb.at[t, 0], f_ss.at[t, 0], f_rs.at[t, 0], xdev(1)).wait_send()
        copy(sb.at[t, 2], fb.at[t, 1], f_ss.at[t, 1], f_rs.at[t, 1], xdev(3)).wait_send()


def on_device(residual_in, queries, keys, values, query_gain, key_norm_gain, out_weight, mlp_gain, gate_weight, up_weight, down_weight):
    tables = [jnp.asarray(t) for t in rotary_tables()]
    dma = pltpu.SemaphoreType.DMA
    vm = pltpu.VMEM
    scratch = [
        vm((2, 16, 6, 128, 128), BF16),
        vm((16, 128, 2 * FF_DEV), BF16),
        vm((16, 768, 128), BF16),
        vm((8, ROWS, HEAD), BF16),
        vm((8, HEAD, 256), BF16),
        vm((CHUNKS, 8, XR, 256), BF16),
        vm((CHUNKS, CT, 768), BF16),
        vm((CHUNKS, 4, CT, 256), BF16),
        vm((CHUNKS, 4, CT, 256), BF16),
        vm((CHUNKS, 4, CT, 256), BF16),
        vm((CHUNKS, 3, CT, 256), BF16),
        vm((CHUNKS, 2, 128, 256), BF16),
        vm((CHUNKS, 2, CT, 256), BF16),
        vm((ROWS, 256), F32),
        vm((HEAD, ROWS), BF16),
        vm((1, ROWS), F32),
        vm((HEAD + 16, ROWS), F32),
        dma((2,)), dma((2, 16)), dma((4,)), dma((4, 16)), dma, dma((16,)), dma, dma((8,)),
        dma((2,)), dma((8,)), dma, dma((4,)),
        dma((CHUNKS, 2)), dma((CHUNKS, 8)), dma((CHUNKS,)), dma((CHUNKS, 4)),
        dma((CHUNKS,)), dma((CHUNKS,)), dma((CHUNKS, 2)), dma((CHUNKS, 2)), dma((CHUNKS, 2)), dma((CHUNKS, 2)),
    ]
    return pl.pallas_call(
        kernel,
        out_shape=jax.ShapeDtypeStruct((ROWS, 256), BF16),
        in_specs=[pl.BlockSpec(memory_space=pltpu.VMEM)] * 15,
        out_specs=pl.BlockSpec(memory_space=pltpu.VMEM),
        scratch_shapes=scratch,
        compiler_params=pltpu.CompilerParams(collective_id=0, has_side_effects=True, vmem_limit_bytes=60 * 1024 * 1024),
        name="layer",
    )(
        residual_in, queries, keys, values, query_gain.reshape(1, HEAD), key_norm_gain.reshape(1, HEAD), out_weight,
        mlp_gain.reshape(1, D), gate_weight, up_weight, down_weight, *tables,
    )


def solution(mesh):
    in_specs = (
        P("sp", "tp"), P("sp", "tp"), P("sp", None), P("sp", None), P(), P(), P("tp", None), P(),
        P("sp", "tp"), P("sp", "tp"), P("tp", "sp"),
    )
    return jax.shard_map(on_device, mesh=mesh, in_specs=in_specs, out_specs=P("sp", "tp"), check_vma=False)
```

time: 338 us -> 129 us (0.38)
  waiting for transfers between devices: 151 us -> 0 us
  Pallas kernels: 0 us -> 124 us
  matrix products: 61.1 us -> 0 us
  blocking collectives: 43.5 us -> 0 us
  other arithmetic: 34.3 us -> 0 us
  starting transfers between devices: 15.5 us -> 0 us
  local copies, waits for them, and re-layouts: 18.2 us -> 4.37 us
  between operations: 13.4 us -> 0.01 us
    all_gather x4 -> x0, waiting for transfers between devices: 128 us -> none  [the longest x2 56.8 us: sent_together(): lax.all_gather(both, axis, axis=dim, tiled=True)]
    pallas_call x0 -> x1, Pallas kernels: none -> 124 us  [on_device(): pl.pallas_call(kernel, out_shape=jax.ShapeDtypeStruct((ROWS, 256), BF16),...]
    dot_general x22 -> x0, matrix products: 61.1 us -> none  [the longest x6 28 us: one_block(): jnp.dot(query_matrix, block_keys.T, preferred_element_type=jnp.float32)]
    all_to_all x1 -> x0, blocking collectives: 43.5 us -> none  [summed_on_arrival(): lax.all_to_all(tiles, axis, split_axis=0, concat_axis=0, tiled=True)]
    reduce_sum x10 -> x0, other arithmetic: 27.5 us -> none  [the longest x6 24.8 us: one_block(): running_sum = running_sum * factor + jnp.sum(weights, axis=1)]
    all_to_all x3 -> x0, waiting for transfers between devices: 22.6 us -> none  [the longest x2 22.6 us: sent_to_all(): lax.all_to_all(jnp.broadcast_to(x[None], (size, *x.shape)), axis, 0, 0, t...]
    all_to_all x3 -> x0, starting transfers between devices: 15.2 us -> none  [the longest x2 9.46 us: sent_to_all(): lax.all_to_all(jnp.broadcast_to(x[None], (size, *x.shape)), axis, 0, 0, t...]
    split x1 -> x0, local copies, waits for them, and re-layouts: 4.7 us -> none  [sent_together(): jnp.split(lax.all_gather(both, axis, axis=dim, tiled=True), ends, axis=al...]
  transfers between devices with their start and end apart: 7 -> 0, of which waited for: 5 -> 0; matrix products, arithmetic and copies ran while one was open for 26% -> 0% of each run, Pallas kernels for 0% -> 0%
where the time goes in v1:
time: 129 us; the launch traced here: 128 us
  Pallas kernels  124 us (96%)
  local copies, waits for them, and re-layouts  4.37 us (3%)
    pallas_call x1, Pallas kernels, on_device(): pl.pallas_call(kernel, out_shape=jax.ShapeDtypeStruct((ROWS, 256), BF16),...  124 us
    unnamed x5, local copies, waits for them, and re-layouts  4.37 us

profile of v1, /device:TPU:1, one launch (start us, length us, event | category | flops | bytes accessed | tf_op | source)
XLA Modules:
  0.0 128.0 jit_solution(17359979093598987719)
XLA Ops:
  0.0 0.0 copy-start
  0.0 1.8 %copy.16.g_ref = bf16[128,704]{1,0:T(8,128)(2,1)} copy(bf16[128,704]{0,1:T(8,128)(2,1)} %param.23) | data formatting | bytes 360448 | tf_op args[8]
  1.8 0.0 copy-done
  1.8 0.8 copy.17.u_ref
  2.6 123.6 %layer.1 = bf16[768,256]{1,0:T(8,128)(2,1)} custom-call(bf16[768,256]{1,0:T(8,128)(2,1)} %res_ref.1, bf16[768,128]{1,0:T(8,128)(2,1)} %q_ref.1, bf16[768,256]{1,0:T(8,128)(2,1)} %k_ref.1, bf16[768,256]{1,0:T(8,128)(2,1)} %v_ref.1, f32[1,128]{1,0:T(1,128)} %bitcast.4, f32[1,128]{1,0:T(1,128)} %bitcast.5, bf16[128,2048]{1,0:T(8,128)(2,1)} %wo_ref.1, ...), custom_call_target="tpu_custom_call" | custom-call | tf_op jit(solution)/shard_map/layer/pallas_call | solution.py:476
  126.2 1.8 %copy.19 = bf16[768,256]{1,0:T(8,128)(2,1)} copy(bf16[768,256]{1,0:T(8,128)(2,1)} %layer.1) | data formatting | bytes 786432
Async XLA Ops:
  0.0 1.8 %copy-start = (bf16[128,704]{0,1:T(8,128)(2,1)S(1)}, bf16[128,704]{0,1:T(8,128)(2,1)}, u32[]{:S(2)}) copy-start(bf16[128,704]{0,1:T(8,128)(2,1)} %param.24) | copy-start | bytes 540676

commit v2 on v1

--- a/solution.py
+++ b/solution.py
@@ -24,9 +24,36 @@
 F32 = jnp.float32
 BF16 = jnp.bfloat16
 
-ORDER = [(0, 0), (0, 3), (3, 0), (0, 1), (1, 0), (0, 2), (2, 0), (3, 3), (3, 1), (1, 3), (1, 1), (3, 2), (2, 3), (1, 2), (2, 1), (2, 2)]
-LOOK = 2
-GU_AT = 10
+ORDER = [(0, 0), (0, 1), (0, 3), (1, 0), (3, 0), (1, 1), (0, 2), (3, 1), (1, 3), (2, 0), (1, 2), (3, 3), (3, 2), (2, 3), (2, 1), (2, 2)]
+SCHEDULE = {
+    "a1": (("ka", 0, 1), ("ka", 0, 3), ("ka", 1, 0), ("ka", 3, 0), ("kb", 0, 1), ("r", 0, 1), ("kb", 0, 3), ("r", 0, 3), ("kb", 1, 0), ("r", 1, 0), ("kb", 3, 0), ("r", 3, 0),),
+    "a2": (("ka", 0, 2), ("ka", 1, 1), ("ka", 3, 1),),
+    "a3": (("kb", 1, 1), ("r", 1, 1), ("ka", 1, 3), ("ka", 3, 3), ("kb", 0, 2), ("r", 0, 2),),
+    "a5": (("kb", 3, 1), ("r", 3, 1), ("ka", 2, 0), ("kb", 1, 3), ("r", 1, 3), ("kb", 2, 0), ("r", 2, 0), ("o", "ga", 0, 1), ("o", "gb", 1, 0),),
+    "a6": (("kb", 1, 2), ("ka", 1, 2), ("r", 1, 2), ("ka", 3, 2), ("kb", 3, 3), ("r", 3, 3), ("o", "ga", 1, 0),),
+    "a7": (("o", "ga", 3, 0), ("o", "ga", 0, 3), ("o", "gb", 0, 1),),
+    "a8": (("ka", 2, 1), ("kb", 3, 2), ("r", 3, 2), ("kb", 2, 3), ("ga", 3, 0), ("o", "gb", 3, 0), ("o", "gb", 0, 3),),
+    "a9": (("ka", 2, 3), ("r", 2, 3), ("gb", 3, 0), ("kb", 2, 1), ("r", 2, 1), ("ga", 0, 3),),
+    "a10": (("ga", 1, 0), ("o", "gc", 0, 3),),
+    "a11": (("ka", 2, 2), ("gb", 0, 3), ("ga", 0, 1), ("o", "gc", 3, 0),),
+    "a12": (("kb", 2, 2), ("r", 2, 2), ("gb", 1, 0), ("ga", 2, 0), ("gb", 0, 1),),
+    "a13": (("ga", 1, 3), ("gb", 2, 0), ("gb", 3, 1), ("gb", 3, 3), ("o", "gc", 0, 1),),
+    "a14": (("gc", 1, 0), ("o", "gd", 3, 0),),
+    "a15": (("ga", 3, 3), ("ga", 0, 2), ("gc", 0, 1),),
+    "p0": (("ga", 1, 1), ("ga", 3, 1), ("gb", 1, 1), ("gb", 0, 2), ("o", "gc", 1, 0),),
+    "p1": (("ga", 2, 3), ("gb", 2, 1), ("gb", 1, 3), ("gc", 3, 0), ("o", "gd", 0, 1), ("gd", 1, 0), ("ga", 3, 2), ("gb", 3, 2), ("gb", 2, 3), ("ga", 1, 2),),
+    "p2": (("gc", 3, 1), ("gc", 0, 2), ("gc", 0, 3), ("o", "gd", 0, 3), ("gc", 1, 1), ("gb", 1, 2), ("gc", 2, 0), ("gd", 0, 3), ("ga", 2, 1),),
+    "p3": (("ga", 2, 2), ("gd", 1, 1), ("gd", 1, 3), ("o", "gd", 1, 0),),
+    "p4": (("gb", 2, 2), ("gd", 2, 0), ("gc", 3, 2), ("gd", 0, 1), ("gc", 1, 2), ("gc", 3, 3), ("gd", 1, 2), ("gd", 0, 2),),
+    "p5": (("gc", 1, 3), ("gd", 3, 0), ("gd", 2, 1), ("gd", 2, 3), ("o", "da", 3, 0), ("o", "da", 0, 1), ("o", "da", 0, 3), ("o", "db", 1, 0), ("gc", 2, 1), ("o", "db", 3, 0), ("gc", 2, 2), ("o", "da", 1, 0), ("o", "db", 0, 3), ("gc", 2, 3), ("gd", 3, 1), ("gd", 3, 3), ("o", "db", 0, 1), ("da", 3, 0), ("da", 1, 0), ("gd", 2, 2), ("da", 0, 1), ("db", 3, 0), ("db", 1, 0), ("da", 0, 3), ("db", 0, 1),),
+    "p7": (("da", 2, 0), ("gd", 3, 2), ("db", 0, 3), ("da", 1, 1),),
+    "p9": (("da", 3, 1), ("da", 0, 2), ("db", 3, 3), ("da", 1, 3), ("db", 2, 0),),
+    "p11": (("db", 1, 3), ("db", 3, 1), ("da", 2, 1), ("da", 3, 3),),
+    "p13": (("db", 0, 2), ("db", 1, 1), ("da", 1, 2), ("da", 3, 2), ("db", 2, 1), ("db", 2, 3),),
+    "p14": (("da", 2, 3), ("db", 3, 2),),
+    "p15": (("db", 1, 2), ("da", 2, 2), ("db", 2, 2),),
+}
+MIRRORED = ("kb", "gc", "gd", "da")
 
 
 def rotary_tables():
@@ -72,13 +99,6 @@
     def copy(src, dst, ss, rs, dev):
         return pltpu.make_async_remote_copy(src_ref=src, dst_ref=dst, send_sem=ss, recv_sem=rs, device_id=dev, device_id_type=MESH)
 
-    def when(cond, fn):
-        if isinstance(cond, (bool, np.bool_)):
-            if cond:
-                fn()
-        else:
-            pl.when(cond)(fn)
-
     barrier = pltpu.get_barrier_semaphore()
     peers = [near(0, 1), near(0, 3), near(1, 0), near(3, 0)]
     peers += [{"sp": sp, "tp": (tp + d) % 8} for d in range(1, 8)]
@@ -102,71 +122,61 @@
         vi = v_ref[i * 128 : (i + 1) * 128, pl.ds(lane0, HEAD)].astype(F32)
         kv[1, sp, i] = vi.T.astype(BF16)
 
-    pl.semaphore_wait(barrier, len(peers))
-
-    def gather(piece, ss, rs, first):
-        def send(a, b, dz, dy):
-            at = ((a - dz + 4) % 4) * 4 + (b - dy + 4) % 4
-            ref = piece(bid(a, b))
-            copy(ref, ref, ss, rs.at[at], near(dz, dy)).start()
-
-        def step(a, b, own=False):
-            u, w = (b, a) if first == "y" else (a, b)
-            if not own:
-                ref = piece(bid(a, b))
-                copy(ref, ref, ss, rs.at[a * 4 + b], near(0, 1)).wait_recv()
-
-            def go(du, dw):
-                dz, dy = (dw, du) if first == "y" else (du, dw)
-                return lambda: send(a, b, dz, dy)
-
-            if own:
-                for du, dw in ((1, 0), (3, 0), (0, 1), (0, 3)):
-                    go(du, dw)()
-            else:
-                even = u % 2 == 0
-                if isinstance(u, int):
-                    when(w == 0 and u == 3, go(1, 0))
-                    when(w == 0 or (w == 3 and even), go(0, 1))
-                    when(w == 0 or (w == 1 and not even), go(0, 3))
+    with jax.named_scope("barrier"):
+        pl.semaphore_wait(barrier, len(peers))
+
+    pieces = {
+        "ka": (lambda i: kv.at[core, i, 0:3], kv_ss.at[0], kv_rs.at[0]),
+        "kb": (lambda i: kv.at[core, i, 3:6], kv_ss.at[1], kv_rs.at[1]),
+        "da": (lambda i: dn.at[i, 0:352], w_ss.at[4], w_rs.at[4]),
+        "db": (lambda i: dn.at[i, 352:704], w_ss.at[5], w_rs.at[5]),
+    }
+    for n, name in enumerate(("ga", "gb", "gc", "gd")):
+        pieces[name] = (lambda i, n=n: gu.at[i, n * 32 : (n + 1) * 32], w_ss.at[n], w_rs.at[n])
+
+    def send(name, a, b, du, dw):
+        piece, ss, rs = pieces[name]
+        dz, dy = (dw, du) if name[1] in "ac" else (du, dw)
+        ref = piece(bid(a, b))
+        copy(ref, ref, ss, rs.at[((a - dz) % 4) * 4 + (b - dy) % 4], near(dz, dy)).start()
+
+    def take(name, a, b):
+        piece, ss, rs = pieces[name]
+        ref = piece(bid(a, b))
+        copy(ref, ref, ss, rs.at[a * 4 + b], near(0, 1)).wait_recv()
+        u, w = (b, a) if name[1] in "ac" else (a, b)
+        if w == 0 and u == 3 and name not in MIRRORED:
+            send(name, a, b, 1, 0)
+        if w == 0 and u == 1 and name in MIRRORED:
+            send(name, a, b, 3, 0)
+        if w == 0 or (w == 3 and u % 2 == 0):
+            send(name, a, b, 0, 1)
+        if w == 0 or (w == 1 and u % 2 == 1):
+            send(name, a, b, 0, 3)
+
+    def drain(name):
+        piece, ss, rs = pieces[name]
+        ref = piece(pl.ds(0, 15))
+        copy(ref, ref, ss, rs.at[0], near(0, 1)).wait_send()
+
+    def run(gap):
+        with jax.named_scope(f"run_{gap}"):
+            for item in SCHEDULE.get(gap, ()):
+                if item[0] == "o":
+                    send(item[1], 0, 0, item[2], item[3])
+                elif item[0] == "r":
+                    ref = kv.at[core, bid(item[1], item[2])]
+                    copy(ref, ref, rel_ss, rel_rs.at[item[1] * 4 + item[2]], partner).start()
                 else:
-                    when((w == 0) & (u == 3), go(1, 0))
-                    when((w == 0) | ((w == 3) & even), go(0, 1))
-                    when((w == 0) | ((w == 1) & (u % 2 == 1)), go(0, 3))
-
-        def drain():
-            ref = piece(pl.ds(0, 15))
-            copy(ref, ref, ss, rs.at[0], near(0, 1)).wait_send()
-
-        return step, drain
-
-    kv_a = gather(lambda i: kv.at[core, i, 0:3], kv_ss.at[0], kv_rs.at[0], "y")
-    kv_b = gather(lambda i: kv.at[core, i, 3:6], kv_ss.at[1], kv_rs.at[1], "z")
-    gu_a = gather(lambda i: gu.at[i, 0:64], w_ss.at[0], w_rs.at[0], "y")
-    gu_b = gather(lambda i: gu.at[i, 64:128], w_ss.at[1], w_rs.at[1], "z")
-    dn_a = gather(lambda i: dn.at[i, 0:352], w_ss.at[2], w_rs.at[2], "y")
-    dn_b = gather(lambda i: dn.at[i, 352:704], w_ss.at[3], w_rs.at[3], "z")
-
-    def kv_step(a, b):
-        kv_a[0](a, b)
-        kv_b[0](a, b)
-        ref = kv.at[core, bid(a, b)]
-        copy(ref, ref, rel_ss, rel_rs.at[a * 4 + b], partner).start()
+                    take(*item)
 
     def kv_relayed(a, b):
         ref = kv.at[1 - core, bid(a, b)]
         copy(ref, ref, rel_ss, rel_rs.at[a * 4 + b], partner).wait_recv()
 
-    def gu_step(a, b, own=False):
-        gu_a[0](a, b, own)
-        gu_b[0](a, b, own)
-
-    def dn_step(a, b, own=False):
-        dn_a[0](a, b, own)
-        dn_b[0](a, b, own)
-
-    kv_a[0](0, 0, True)
-    kv_b[0](0, 0, True)
+    for name in ("ka", "kb"):
+        for du, dw in ((1, 0), (3, 0), (0, 1), (0, 3)):
+            send(name, 0, 0, du, dw)
 
     for d in range(1, 8):
         to = (tp + d) % 8
@@ -180,9 +190,10 @@
     acc[...] = jnp.zeros_like(acc)
 
     for n in range(5):
-        gu[sp, :, n * 256 : n * 256 + 128] = g_ref[:, n * 128 : (n + 1) * 128]
-        gu[sp, :, n * 256 + 128 : (n + 1) * 256] = u_ref[:, n * 128 : (n + 1) * 128]
-    gu[sp, :, 1280:1408] = jnp.concatenate([g_ref[:, 640:704], u_ref[:, 640:704]], axis=1)
+        cols = slice(n * 128, (n + 1) * 128)
+        gu[sp, :, n * 256 : n * 256 + 128] = g_ref[cols, :].T
+        gu[sp, :, n * 256 + 128 : (n + 1) * 256] = u_ref[cols, :].T
+    gu[sp, :, 1280:1408] = jnp.concatenate([g_ref[640:704, :], u_ref[640:704, :]], axis=0).T
     dn[sp, 0:704, :] = dw_ref[...]
     for i in range(16):
         dn[i, 704:768, :] = jnp.zeros((64, 128), BF16)
@@ -208,44 +219,25 @@
             b = jnp.where(s == i, bi, b)
         return a, b
 
-    attend(sp)
-    for i in range(1, 1 + LOOK):
-        kv_step(*ORDER[i])
+    run("own")
+    with jax.named_scope("att_own"):
+        attend(sp)
 
     def att_loop(s, c):
-        @pl.when(s + LOOK < 16)
-        def _():
-            kv_step(*place(s + LOOK))
-
-        @pl.when(s == GU_AT)
-        def _():
-            gu_step(0, 0, True)
-
-        @pl.when(s > GU_AT)
-        def _():
-            gu_step(*place(s - GU_AT))
-
+        for i in range(1, 16):
+            pl.when(s == i)(functools.partial(run, f"a{i}"))
         a, b = place(s)
-        kv_relayed(a, b)
-        attend(bid(a, b))
+        with jax.named_scope("relay_wait"):
+            kv_relayed(a, b)
+        with jax.named_scope("attend"):
+            attend(bid(a, b))
         return c
 
     lax.fori_loop(1, 16, att_loop, 0)
-
-    todo = [functools.partial(gu_step, *ORDER[i]) for i in range(16 - GU_AT, 11)]
-    todo += [functools.partial(dn_step, 0, 0, True)]
-    todo += [functools.partial(gu_step, *ORDER[i]) for i in range(11, 16)]
-    gu_left = len(todo)
-    todo += [functools.partial(dn_step, *ORDER[i]) for i in range(1, 16)]
-    done = [0]
-
-    def pump(upto):
-        while done[0] < upto:
-            todo[done[0]]()
-            done[0] += 1
-
-    attn = (acc[0:HEAD, :] / acc[HEAD : HEAD + 1, :]).T.astype(BF16)
-    att[tp] = attn
+    run("p0")
+    with jax.named_scope("att_out"):
+        attn = (acc[0:HEAD, :] / acc[HEAD : HEAD + 1, :]).T.astype(BF16)
+        att[tp] = attn
 
     def xgather(block, pieces, ss, rs, dss, drs):
         def own(dx):
@@ -309,15 +301,20 @@
         xgather(rows_of(xn.at[t]), ((0, 128), (128, XR)), xs_ss.at[t], xs_rs.at[t], xd_ss.at[t], xd_rs.at[t])
         for t in range(CHUNKS)
     ]
-    at_x[0]()
-    pump(2)
-    at_x[1]()
+    with jax.named_scope("at_x0"):
+        at_x[0]()
+    run("p1")
+    with jax.named_scope("at_x1"):
+        at_x[1]()
     for d in range(1, 8):
         frm = (tp + d) % 8
         copy(wo.at[frm], wo.at[frm], wo_ss, wo_rs.at[d], {"sp": sp, "tp": frm}).wait_recv()
-    pump(4)
-    at_x[2]()
-    at_x[3]()
+    run("p2")
+    with jax.named_scope("at_x2"):
+        at_x[2]()
+    run("p3")
+    with jax.named_scope("at_x3"):
+        at_x[3]()
 
     mgain = mg_ref[:, pl.ds(pl.multiple_of(tp * 256, 256), 256)]
 
@@ -332,9 +329,10 @@
         row = lax.broadcasted_iota(jnp.int32, (16, CT), 0)
         xn[t, tp, CT:XR, :] = jnp.where(row == 0, hi, jnp.where(row == 1, sq - hi, 0.0)).astype(BF16)
 
-    for t in range(CHUNKS):
-        project(t)
-        xn_x[t][0]()
+    with jax.named_scope("project"):
+        for t in range(CHUNKS):
+            project(t)
+            xn_x[t][0]()
 
     def gate_up(t):
         total = jnp.zeros((16, CT), F32)
@@ -401,42 +399,75 @@
         total = both(t, 0) + fb[t, 0].astype(F32) + fb[t, 1].astype(F32)
         out_ref[rows, :] = (rm[rows, :] + 0.5 * total).astype(BF16)
 
-    pump(gu_left - 3)
-    xn_x[0][1]()
-    pump(gu_left)
-    xn_x[0][2]()
-    xn_x[1][1]()
-    xn_x[0][3]()
-    gate_up(0)
-    pump(gu_left + 5)
-    xn_x[1][2]()
-    xn_x[2][1]()
-    xn_x[1][3]()
-    gate_up(1)
-    pump(gu_left + 10)
-    xn_x[2][2]()
-    xn_x[2][3]()
-    gate_up(2)
-    pump(len(todo))
-    down(0)
-    reduce_far(0)
-    down(1)
-    reduce_near(0)
-    reduce_far(1)
-    down(2)
-    reduce_near(1)
-    reduce_far(2)
-    final(0)
-    reduce_near(2)
-    final(1)
-    final(2)
-
-    for _, drain in (kv_a, kv_b, gu_a, gu_b, dn_a, dn_b):
-        drain()
+    run("p4")
+    with jax.named_scope("xn_x01"):
+        xn_x[0][1]()
+    run("p5")
+    with jax.named_scope("xn_x02"):
+        xn_x[0][2]()
+    run("p6")
+    with jax.named_scope("xn_x11"):
+        xn_x[1][1]()
+    run("p7")
+    with jax.named_scope("xn_x03"):
+        xn_x[0][3]()
+    run("p8")
+    with jax.named_scope("gate_up0"):
+        gate_up(0)
+    run("p9")
+    with jax.named_scope("xn_x12"):
+        xn_x[1][2]()
+    run("p10")
+    with jax.named_scope("xn_x21"):
+        xn_x[2][1]()
+    run("p11")
+    with jax.named_scope("xn_x13"):
+        xn_x[1][3]()
+    run("p12")
+    with jax.named_scope("gate_up1"):
+        gate_up(1)
+    run("p13")
+    with jax.named_scope("xn_x22"):
+        xn_x[2][2]()
+    run("p14")
+    with jax.named_scope("xn_x23"):
+        xn_x[2][3]()
+    with jax.named_scope("gate_up2"):
+        gate_up(2)
+    run("p15")
+    with jax.named_scope("down0"):
+        down(0)
+    with jax.named_scope("reduce_far0"):
+        reduce_far(0)
+    with jax.named_scope("down1"):
+        down(1)
+    with jax.named_scope("reduce_near0"):
+        reduce_near(0)
+    with jax.named_scope("reduce_far1"):
+        reduce_far(1)
+    with jax.named_scope("down2"):
+        down(2)
+    with jax.named_scope("reduce_near1"):
+        reduce_near(1)
+    with jax.named_scope("reduce_far2"):
+        reduce_far(2)
+    with jax.named_scope("final0"):
+        final(0)
+    with jax.named_scope("reduce_near2"):
+        reduce_near(2)
+    with jax.named_scope("final1"):
+        final(1)
+    with jax.named_scope("final2"):
+        final(2)
+
+    with jax.named_scope("drain"):
+        for name in pieces:
+            drain(name)
     ref = kv.at[0, 0:15]
     copy(ref, ref, rel_ss, rel_rs.at[0], partner).wait_send()
     copy(wo.at[0:7], wo.at[0:7], wo_ss, wo_rs.at[0], partner).wait_send()
-    at_x[4]()
+    with jax.named_scope("at_x4"):
+        at_x[4]()
     for t in range(CHUNKS):
         xn_x[t][4]()
         copy(tb.at[t], rb.at[t], td_ss.at[t], td_rs.at[t], partner).wait_send()
@@ -468,7 +499,7 @@
         vm((HEAD, ROWS), BF16),
         vm((1, ROWS), F32),
         vm((HEAD + 16, ROWS), F32),
-        dma((2,)), dma((2, 16)), dma((4,)), dma((4, 16)), dma, dma((16,)), dma, dma((8,)),
+        dma((2,)), dma((2, 16)), dma((6,)), dma((6, 16)), dma, dma((16,)), dma, dma((8,)),
         dma((2,)), dma((8,)), dma, dma((4,)),
         dma((CHUNKS, 2)), dma((CHUNKS, 8)), dma((CHUNKS,)), dma((CHUNKS, 4)),
         dma((CHUNKS,)), dma((CHUNKS,)), dma((CHUNKS, 2)), dma((CHUNKS, 2)), dma((CHUNKS, 2)), dma((CHUNKS, 2)),
@@ -483,7 +514,7 @@
         name="layer",
     )(
         residual_in, queries, keys, values, query_gain.reshape(1, HEAD), key_norm_gain.reshape(1, HEAD), out_weight,
-        mlp_gain.reshape(1, D), gate_weight, up_weight, down_weight, *tables,
+        mlp_gain.reshape(1, D), gate_weight.T, up_weight.T, down_weight, *tables,
     )
 
 

time: 129 us -> 106 us (0.82)
  Pallas kernels: 124 us -> 103 us
  local copies, waits for them, and re-layouts: 4.37 us -> 1.77 us
    pallas_call x1, Pallas kernels: 124 us -> 103 us  [on_device(): pl.pallas_call(kernel, out_shape=jax.ShapeDtypeStruct((ROWS, 256), BF16),...]
    unnamed x5 -> x1, local copies, waits for them, and re-layouts: 4.37 us -> 1.77 us
where the time goes in v2:
time: 106 us; the launch traced here: 105 us
  Pallas kernels  103 us (97%)
  local copies, waits for them, and re-layouts  1.77 us (2%)
    pallas_call x1, Pallas kernels, on_device(): pl.pallas_call(kernel, out_shape=jax.ShapeDtypeStruct((ROWS, 256), BF16),...  103 us

profile of v2, /device:TPU:1, one launch (start us, length us, event | category | flops | bytes accessed | tf_op | source)
XLA Modules:
  0.0 105.0 jit_solution(16040745417245992956)
XLA Ops:
  0.0 103.2 %layer.1 = bf16[768,256]{1,0:T(8,128)(2,1)} custom-call(bf16[768,256]{1,0:T(8,128)(2,1)} %res_ref.1, bf16[768,128]{1,0:T(8,128)(2,1)} %q_ref.1, bf16[768,256]{1,0:T(8,128)(2,1)} %k_ref.1, bf16[768,256]{1,0:T(8,128)(2,1)} %v_ref.1, f32[1,128]{1,0:T(1,128)} %bitcast.8, f32[1,128]{1,0:T(1,128)} %bitcast.9, bf16[128,2048]{1,0:T(8,128)(2,1)} %wo_ref.1, ...), custom_call_target="tpu_custom_call" | custom-call | tf_op jit(solution)/shard_map/layer/pallas_call | solution.py:507
  103.2 1.8 %copy.17 = bf16[768,256]{1,0:T(8,128)(2,1)} copy(bf16[768,256]{1,0:T(8,128)(2,1)} %layer.1) | data formatting | bytes 786432

commit v3 on v2

v3 whole, which is shorter than its diff:
```python
import functools
import math

import jax
import jax.numpy as jnp
import numpy as np
from jax import lax
from jax.experimental import pallas as pl
from jax.experimental.pallas import tpu as pltpu
from jax.sharding import PartitionSpec as P

D = 2048
HEAD = 128
GRID = 64
ROWS = 768
FF_DEV = 704
EPS = 1e-06
TT = ROWS // 8
HALF = ROWS // 2

LOG2E = 1.4426950408889634
SCORE = HEAD ** (-0.5) * LOG2E
MESH = pl.DeviceIdType.MESH
F32 = jnp.float32
BF16 = jnp.bfloat16

ORDER = [(0, 0), (3, 0), (1, 0), (0, 1), (0, 3), (3, 3), (2, 0), (1, 3), (1, 1), (0, 2), (3, 1), (3, 2), (2, 3), (2, 1), (1, 2), (2, 2)]
SCHEDULE = {
    "own": (("o", "gd", 1, 0), ("o", "gd", 0, 3),),
    "a1": (("ka", 0, 3), ("ka", 3, 0), ("ka", 0, 1), ("ka", 1, 0), ("o", "ga", 3, 0), ("kb", 3, 0), ("r", 3, 0), ("kb", 1, 0), ("r", 1, 0), ("kb", 0, 1), ("r", 0, 1), ("kb", 0, 3), ("r", 0, 3),),
    "a3": (("ka", 0, 2), ("ka", 1, 3), ("gd", 0, 1), ("gd", 3, 0),),
    "a4": (("ka", 3, 3), ("ga", 0, 1),),
    "a5": (("ka", 1, 1), ("kb", 3, 3), ("r", 3, 3), ("kb", 3, 1), ("ka", 2, 0), ("kb", 2, 0), ("r", 2, 0), ("kb", 1, 3), ("r", 1, 3),),
    "a6": (("o", "gc", 0, 1),),
    "a7": (("kb", 1, 1), ("r", 1, 1), ("kb", 0, 2), ("r", 0, 2), ("ka", 3, 1), ("r", 3, 1), ("ka", 1, 2), ("o", "gd", 0, 1),),
    "a8": (("gd", 3, 1), ("ka", 3, 2), ("o", "ga", 1, 0),),
    "a9": (("ka", 2, 3), ("gd", 3, 3), ("o", "gd", 3, 0),),
    "a10": (("kb", 3, 2), ("r", 3, 2), ("ga", 3, 1), ("o", "gb", 3, 0), ("o", "gb", 1, 0),),
    "a11": (("ga", 1, 1), ("kb", 2, 3), ("r", 2, 3),),
    "a12": (("kb", 2, 1), ("gd", 0, 3), ("ka", 2, 1), ("r", 2, 1), ("gc", 3, 0), ("o", "gc", 3, 0),),
    "a13": (("o", "ga", 0, 1), ("kb", 1, 2), ("r", 1, 2), ("ka", 2, 2), ("o", "ga", 0, 3), ("o", "gc", 1, 0),),
    "a14": (("gd", 1, 0), ("ga", 0, 3),),
    "a15": (("gb", 3, 0), ("kb", 2, 2), ("r", 2, 2), ("gb", 1, 0), ("gd", 3, 2),),
    "p0": (("gc", 2, 0), ("ga", 2, 1), ("gc", 0, 1), ("gd", 0, 2),),
    "p1": (("gd", 1, 1), ("ga", 3, 0), ("gc", 0, 3), ("ga", 1, 0),),
    "p2": (("ga", 3, 3), ("gb", 3, 1), ("gd", 2, 0), ("gd", 1, 3), ("gb", 2, 0), ("gb", 1, 1), ("ga", 0, 2), ("ga", 1, 3), ("gc", 3, 1), ("gc", 0, 2), ("gb", 3, 3), ("gc", 1, 1),),
    "p4": (("gd", 1, 2), ("ga", 2, 0), ("gb", 1, 3), ("gc", 1, 3), ("o", "gb", 0, 1), ("o", "db", 1, 0), ("gc", 3, 3), ("gb", 3, 2), ("o", "da", 3, 0), ("ga", 1, 2), ("gd", 2, 3), ("ga", 3, 2), ("gd", 2, 1), ("ga", 2, 3), ("gb", 2, 3), ("gc", 3, 2), ("gb", 2, 1), ("o", "gb", 0, 3), ("o", "gc", 0, 3), ("o", "db", 3, 0), ("gb", 0, 3), ("gc", 1, 2),),
    "p5": (("o", "da", 1, 0), ("o", "db", 0, 1),),
    "p6": (("db", 3, 0), ("gb", 1, 2), ("gc", 2, 1), ("gd", 2, 2), ("ga", 2, 2), ("da", 0, 1), ("o", "da", 0, 3), ("gb", 2, 2), ("gc", 2, 3),),
    "p7": (("gc", 2, 2), ("gb", 0, 1), ("o", "da", 0, 1), ("gb", 0, 2), ("gc", 1, 0),),
    "g0": (("o", "db", 0, 3),),
    "g1": (("db", 2, 0), ("db", 1, 0), ("db", 3, 1), ("da", 0, 3),),
    "g3": (("da", 0, 2), ("da", 3, 1), ("da", 1, 1), ("db", 0, 3),),
    "p9": (("db", 0, 1), ("da", 3, 0),),
    "i0": (("db", 3, 3), ("da", 1, 0),),
    "p12": (("db", 2, 1), ("da", 3, 3), ("da", 1, 3), ("db", 2, 3), ("da", 3, 2), ("db", 1, 1), ("da", 1, 2), ("db", 1, 3), ("db", 3, 2), ("da", 2, 0), ("da", 2, 1), ("db", 0, 2), ("da", 2, 3), ("da", 2, 2), ("db", 2, 2), ("db", 1, 2),),
}
FAR_AT = 3
MIRRORED = ("kb", "gc", "gd", "da")


def rotary_tables():
    half = HEAD // 2
    freq = (10000.0 ** (-np.arange(0, half, 2, dtype=np.float32) / np.float32(half))).astype(np.float32)
    lanes = np.arange(HEAD)
    of_row = (lanes % 64) < 32
    sign = np.where(lanes < 64, -1.0, 1.0)
    f = freq[lanes % 32]
    out = []
    for count, mask in ((12288 // GRID, of_row), (GRID, ~of_row)):
        ang = (np.arange(count, dtype=np.float32)[:, None] * f[None, :]).astype(np.float32).astype(np.float64)
        out.append(np.where(mask, np.cos(ang), 0.0).astype(np.float32))
        out.append(np.where(mask, np.sin(ang) * sign, 0.0).astype(np.float32))
    return out


def kernel(
    res_h, q_ref, k_ref, v_ref, qg_ref, kg_ref, wo_h, mg_ref, g_h, u_h, dw_h,
    rc_ref, rs_ref, cc_ref, cs_ref,
    out_ref,
    kv, gu, dn, att, att_t, wo, res_t, mid_s, xn, pj, pr, hid, tb, rb, sb, pb, fb, qT, m_s, acc, scores, gu_s, base_s, res_ref, g_ref, u_ref, in_s,
    kv_ss, kv_rs, w_ss, w_rs, rel_ss, rel_rs, wo_ss, wo_rs, wd_ss, wd_rs, res_ss, res_rs, at_ss, at_rs,
    xs_ss, xs_rs, xd_ss, xd_rs, pj_ss, pj_rs, td_ss, td_rs, p_ss, p_rs, f_ss, f_rs,
):
    sp = lax.axis_index("sp")
    tp = lax.axis_index("tp")
    z, y = sp // 4, sp % 4
    x, core = tp // 2, tp % 2

    def bid(a, b):
        return ((z + a) % 4) * 4 + (y + b) % 4

    def near(dz, dy):
        return {"sp": bid(dz, dy), "tp": tp}

    def xdev(dx):
        return {"sp": sp, "tp": ((x + dx) % 4) * 2 + core}

    partner_tp = x * 2 + 1 - core
    partner = {"sp": sp, "tp": partner_tp}

    def copy(src, dst, ss, rs, dev):
        return pltpu.make_async_remote_copy(src_ref=src, dst_ref=dst, send_sem=ss, recv_sem=rs, device_id=dev, device_id_type=MESH)

    barrier = pltpu.get_barrier_semaphore()
    peers = [near(0, 1), near(0, 3), near(1, 0), near(3, 0)]
    peers += [{"sp": sp, "tp": (tp + d) % 8} for d in range(1, 8)]
    for dev in peers:
        pl.semaphore_signal(barrier, inc=1, device_id=dev, device_id_type=MESH)

    loads = [
        pltpu.make_async_copy(res_h, res_ref, in_s.at[0]),
        pltpu.make_async_copy(wo_h, wo.at[tp], in_s.at[1]),
        pltpu.make_async_copy(g_h, g_ref, in_s.at[2]),
        pltpu.make_async_copy(u_h, u_ref, in_s.at[3]),
        pltpu.make_async_copy(dw_h, dn.at[sp, 0:FF_DEV], in_s.at[4]),
    ]
    for load in loads:
        load.start()

    def rotated(ref, lane0, gain, g):
        t = ref[g * 64 : (g + 1) * 64, pl.ds(lane0, HEAD)].astype(F32)
        t = t * lax.rsqrt(jnp.mean(t * t, axis=1, keepdims=True) + EPS) * gain
        grid_row = sp * (ROWS // GRID) + g
        cos = rc_ref[pl.ds(grid_row, 1), :] + cc_ref[...]
        sin = rs_ref[pl.ds(grid_row, 1), :] + cs_ref[...]
        return t * cos + pltpu.roll(t, 64, 1) * sin

    lane0 = pl.multiple_of((tp // 4) * HEAD, HEAD)
    kgain = kg_ref[...]
    qgain = qg_ref[...]
    def own_keys():
        for g in range(ROWS // GRID):
            kv[0, sp, g // 2, pl.ds((g % 2) * 64, 64), :] = rotated(k_ref, lane0, kgain, g).astype(BF16)

    def own_values():
        for i in range(6):
            vi = v_ref[i * 128 : (i + 1) * 128, pl.ds(lane0, HEAD)].astype(F32)
            kv[1, sp, i] = vi.T.astype(BF16)

    pl.when(core == 0)(own_keys)
    pl.when(core == 1)(own_values)

    with jax.named_scope("barrier"):
        pl.semaphore_wait(barrier, len(peers))

    pieces = {
        "ka": (lambda i: kv.at[core, i, 0:3], kv_ss.at[0], kv_rs.at[0]),
        "kb": (lambda i: kv.at[core, i, 3:6], kv_ss.at[1], kv_rs.at[1]),
        "da": (lambda i: dn.at[i, 0:352], w_ss.at[4], w_rs.at[4]),
        "db": (lambda i: dn.at[i, 352:704], w_ss.at[5], w_rs.at[5]),
    }
    for n, name in enumerate(("ga", "gb", "gc", "gd")):
        pieces[name] = (lambda i, n=n: gu.at[i, n * 32 : (n + 1) * 32], w_ss.at[n], w_rs.at[n])

    def send(name, a, b, du, dw):
        piece, ss, rs = pieces[name]
        dz, dy = (dw, du) if name[1] in "ac" else (du, dw)
        ref = piece(bid(a, b))
        copy(ref, ref, ss, rs.at[((a - dz) % 4) * 4 + (b - dy) % 4], near(dz, dy)).start()

    def take(name, a, b):
        piece, ss, rs = pieces[name]
        ref = piece(bid(a, b))
        copy(ref, ref, ss, rs.at[a * 4 + b], near(0, 1)).wait_recv()
        u, w = (b, a) if name[1] in "ac" else (a, b)
        if w == 0 and u == 3 and name not in MIRRORED:
            send(name, a, b, 1, 0)
        if w == 0 and u == 1 and name in MIRRORED:
            send(name, a, b, 3, 0)
        if w == 0 or (w == 3 and u % 2 == 0):
            send(name, a, b, 0, 1)
        if w == 0 or (w == 1 and u % 2 == 1):
            send(name, a, b, 0, 3)

    def drain(name):
        piece, ss, rs = pieces[name]
        ref = piece(pl.ds(0, 15))
        copy(ref, ref, ss, rs.at[0], near(0, 1)).wait_send()

    def run(gap):
        with jax.named_scope(f"run_{gap}"):
            for item in SCHEDULE.get(gap, ()):
                if item[0] == "o":
                    send(item[1], 0, 0, item[2], item[3])
                elif item[0] == "r":
                    ref = kv.at[core, bid(item[1], item[2])]
                    copy(ref, ref, rel_ss, rel_rs.at[item[1] * 4 + item[2]], partner).start()
                else:
                    take(*item)

    def kv_relayed(a, b):
        ref = kv.at[1 - core, bid(a, b)]
        copy(ref, ref, rel_ss, rel_rs.at[a * 4 + b], partner).wait_recv()

    for name in ("ka", "kb"):
        for du, dw in ((1, 0), (3, 0), (0, 1), (0, 3)):
            send(name, 0, 0, du, dw)

    pl.when(core == 1)(own_keys)
    pl.when(core == 0)(own_values)

    def tokens(i):
        return pl.ds(pl.multiple_of(i * TT, TT), TT)

    def exchange(src, dst, ss, rs):
        for d in (1, 2, 7, 6, 3, 5, 4):
            to = (tp + d) % 8
            copy(src(to), dst(tp), ss, rs.at[8 - d], {"sp": sp, "tp": to}).start()

    def exchanged(dst, ss, rs):
        for d in range(1, 8):
            frm = (tp + d) % 8
            copy(dst(frm), dst(frm), ss, rs.at[d], {"sp": sp, "tp": frm}).wait_recv()

    def exchange_drain(dst, ss, rs):
        ref = dst(pl.ds(0, 7))
        copy(ref, ref, ss, rs.at[0], partner).wait_send()

    for load in loads:
        load.wait()
    exchange(lambda i: res_ref.at[tokens(i)], lambda i: res_t.at[i], res_ss, res_rs)

    for g in range(ROWS // GRID):
        qT[:, g * 64 : (g + 1) * 64] = rotated(q_ref, 0, qgain, g).T.astype(BF16)
    m_s[...] = jnp.full_like(m_s, -1e30)
    acc[...] = jnp.zeros_like(acc)

    for n in range(5):
        cols = slice(n * 128, (n + 1) * 128)
        gu[sp, :, n * 256 : n * 256 + 128] = g_ref[cols, :].T
        gu[sp, :, n * 256 + 128 : (n + 1) * 256] = u_ref[cols, :].T
    gu[sp, :, 1280:1408] = jnp.concatenate([g_ref[640:704, :], u_ref[640:704, :]], axis=0).T
    for i in range(16):
        dn[i, 704:768, :] = jnp.zeros((64, 128), BF16)

    def xgather(block, pieces, ss, rs, dss, drs):
        def own(dx):
            return ((x + dx) % 4) * 2 + core

        def send(dx, p, to):
            ref = block(own(dx), pieces[p])
            copy(ref, ref, ss.at[p], rs.at[((dx - to) % 4) * 2 + p], xdev(to)).start()

        def wait(dx, p):
            ref = block(own(dx), pieces[p])
            copy(ref, ref, ss.at[p], rs.at[(dx % 4) * 2 + p], xdev(1)).wait_recv()

        whole = (0, pieces[1][1])

        def relay(dx):
            ref = block(own(dx), whole)
            copy(ref, ref, dss, drs.at[dx % 4], partner).start()

        def start():
            send(0, 0, 1)
            send(0, 1, 3)
            send(0, 1, 1)
            send(0, 0, 3)
            relay(0)

        def forward():
            wait(3, 0)
            send(3, 0, 1)
            wait(1, 1)
            send(1, 1, 3)

        def finish():
            wait(3, 1)
            relay(3)
            wait(1, 0)
            relay(1)

        def finish_far():
            wait(2, 0)
            wait(2, 1)
            relay(2)

        def relayed(which=(0, 3, 1, 2)):
            for dx in which:
                ref = block(((x + dx) % 4) * 2 + 1 - core, whole)
                copy(ref, ref, dss, drs.at[dx], partner).wait_recv()

        def drain():
            for p in range(2):
                ref = block(pl.ds(0, 3), pieces[p])
                copy(ref, ref, ss.at[p], rs.at[0], xdev(1)).wait_send()
            ref = block(pl.ds(0, 4), whole)
            copy(ref, ref, dss, drs.at[0], partner).wait_send()

        return start, forward, finish, finish_far, relayed, drain

    def rows_of(ref):
        return lambda i, r: ref.at[i, r[0] : r[1]]

    wo_start, wo_forward, wo_finish, wo_far, wo_relayed, wo_drain = xgather(
        rows_of(wo), ((0, 64), (64, HEAD)), wo_ss, wo_rs, wd_ss, wd_rs
    )
    xn_start, xn_forward, xn_finish, xn_far, xn_relayed, xn_drain = xgather(
        rows_of(xn), ((0, TT // 2), (TT // 2, TT)), xs_ss, xs_rs, xd_ss, xd_rs
    )
    wo_start()

    def product(blk):
        return jnp.dot(kv[0, blk].reshape(ROWS, HEAD), qT[...], preferred_element_type=F32)

    def absorb(s, blk):
        old = m_s[...]
        new = jnp.maximum(old, jnp.max(s, axis=0, keepdims=True))
        factor = jnp.exp2((old - new) * SCORE)
        m_s[...] = new
        p = jnp.exp2((s - new) * SCORE).astype(BF16)
        v = kv[1, blk]
        vt = jnp.concatenate([v[i] for i in range(6)], axis=1)
        vt = jnp.concatenate([vt, jnp.ones((16, ROWS), BF16)], axis=0)
        acc[...] = acc[...] * factor + jnp.dot(vt, p, preferred_element_type=F32)

    def place(s):
        a, b = jnp.int32(0), jnp.int32(0)
        for i, (ai, bi) in enumerate(ORDER):
            a = jnp.where(s == i, ai, a)
            b = jnp.where(s == i, bi, b)
        return a, b

    run("own")
    with jax.named_scope("att_own"):
        absorb(product(sp), sp)
    run("a1")
    with jax.named_scope("relay_wait"):
        kv_relayed(*ORDER[1])
    with jax.named_scope("first"):
        scores[0] = product(bid(*ORDER[1]))

    def att_loop(i, c):
        for h in range(2):
            s = 2 * i + 1 + h
            for k in range(2 + h, 16, 2):
                pl.when(s == k - 1)(functools.partial(run, f"a{k}"))
            for k, fn in ((3, wo_forward), (9, wo_finish), (13, wo_far)):
                if k % 2 == 1 - h:
                    pl.when(s == k)(fn)
            now, later = place(s), place(s + 1)
            with jax.named_scope("relay_wait"):
                kv_relayed(*later)
            with jax.named_scope("attend"):
                scores[1 - h] = product(bid(*later))
                absorb(scores[h], bid(*now))
        return c

    lax.fori_loop(0, 7, att_loop, 0)
    absorb(scores[0], bid(*ORDER[15]))
    run("p0")
    with jax.named_scope("att_out"):
        attn = (acc[0:HEAD, :] / acc[HEAD : HEAD + 1, :]).T.astype(BF16)
        att[...] = attn

    exchange(lambda i: att.at[tokens(i)], lambda i: att_t.at[i], at_ss, at_rs)
    att_t[tp] = att[tokens(tp)]
    res_t[tp] = res_ref[tokens(tp), :]
    run("p1")
    with jax.named_scope("wo_wait"):
        wo_relayed()
        exchanged(lambda i: res_t.at[i], res_ss, res_rs)
    run("p2")
    with jax.named_scope("att_wait"):
        exchanged(lambda i: att_t.at[i], at_ss, at_rs)

    def project():
        left = jnp.concatenate([att_t[i] for i in range(8)], axis=1)
        squares = jnp.zeros((TT, 1), F32)
        for n in range(4):
            cols = slice(n * 512, (n + 1) * 512)
            p = jnp.dot(left, wo[:, :, cols].reshape(8 * HEAD, 512), preferred_element_type=F32)
            for i in range(2):
                part = p[:, i * 256 : (i + 1) * 256]
                pj[2 * n + i] = part.astype(BF16)
                mid = res_t[2 * n + i].astype(F32) + part
                mid_s[:, n * 512 + i * 256 : n * 512 + (i + 1) * 256] = mid
                squares = squares + jnp.sum(mid * mid, axis=1, keepdims=True)
        scale = lax.rsqrt(squares / D + EPS)
        xn[tp] = (mid_s[...] * scale * mg_ref[...]).astype(BF16)

    with jax.named_scope("project"):
        project()
    xn_start()

    def gate_up(far_by, name):
        chips = [(x + dx) % 4 for dx in far_by]

        def keep(value, lanes):
            for i, c in enumerate(chips):
                rows = pl.ds(pl.multiple_of(c * 2 * TT, 2 * TT), 2 * TT)
                hid[rows, lanes] = value[i * 2 * TT : (i + 1) * 2 * TT].astype(BF16)

        count = len(chips) * 2 * TT

        def silu(n):
            o = gu_s[n % 2, 0:count, :]
            if n < 5:
                gate, up = o[:, 0:128], o[:, 128:256]
                keep(gate / (1.0 + jnp.exp(-gate)) * up, slice(n * 128, (n + 1) * 128))
            else:
                o = o[:, 0:128]
                tail = o / (1.0 + jnp.exp(-o)) * pltpu.roll(o, 64, 1)
                lane = lax.broadcasted_iota(jnp.int32, tail.shape, 1)
                keep(jnp.where(lane < 64, tail, 0.0), slice(640, 768))

        for n in range(6):
            width = 256 if n < 5 else 128
            w = gu[:, :, n * 256 : n * 256 + width].reshape(D, width)
            for i, c in enumerate(chips):
                left = xn[pl.ds(2 * c, 2)].reshape(2 * TT, D)
                gu_s[n % 2, i * 2 * TT : (i + 1) * 2 * TT, 0:width] = jnp.dot(left, w, preferred_element_type=F32)
            if n > 0:
                silu(n - 1)
            if n < 5:
                run(f"{name}{n}")
                if name == "g" and n == FAR_AT:
                    run("gf")
                    with jax.named_scope("xn_far"):
                        xn_far()
        silu(5)

    def down(dx, rows=slice(0, ROWS)):
        j = ((x + dx) % 4) * 4
        w = jnp.concatenate([dn[j + i] for i in range(4)], axis=1)
        o = jnp.dot(hid[rows, :], w, preferred_element_type=F32)
        for c in range(2):
            tb[dx, c, rows] = o[:, c * 256 : (c + 1) * 256].astype(BF16)

    def to_partner(dx):
        return copy(tb.at[dx, 1 - core], rb.at[dx], td_ss.at[dx], td_rs.at[dx], partner)

    def half_to_partner(h):
        rows = pl.ds(h * HALF, HALF)
        return copy(tb.at[2, 1 - core, rows], rb.at[2, rows], td_ss.at[2 + 2 * h], td_rs.at[2 + 2 * h], partner)

    def far(i):
        to = xdev((1, 3)[i])
        return copy(sb.at[0, pl.ds(i * HALF, HALF)], pb.at[i], p_ss.at[i], p_rs.at[i], to)

    def close(i, h):
        to = xdev((1, 3)[i])
        rows = pl.ds(h * HALF, HALF)
        return copy(sb.at[1 + i, rows], fb.at[i, rows], f_ss.at[i, h], f_rs.at[i, h], to)

    def both(dx, h):
        rows = slice(h * HALF, (h + 1) * HALF)
        return tb[dx, core, rows].astype(F32) + rb[dx, rows].astype(F32)

    def reduce_far(i):
        half_to_partner(i).wait_recv()
        sb[0, i * HALF : (i + 1) * HALF] = both(2, i).astype(BF16)
        far(i).start()

    def reduce_free(i):
        dx, h = (1, 3)[i], 1 - i
        to_partner(dx).wait_recv()
        sb[1 + i, h * HALF : (h + 1) * HALF] = both(dx, h).astype(BF16)
        close(i, h).start()

    def reduce_near(i):
        dx, h = (1, 3)[i], i
        s = both(dx, h)
        far(i).wait_recv()
        sb[1 + i, h * HALF : (h + 1) * HALF] = (s + pb[i].astype(F32)).astype(BF16)
        close(i, h).start()

    def begin(h):
        rows = slice(h * HALF, (h + 1) * HALF)
        i = 1 - h
        close(i, h).wait_recv()
        mid = res_ref[rows, :].astype(F32) + pr[h * 4 : h * 4 + 4].reshape(HALF, 256).astype(F32)
        base_s[rows, :] = mid + 0.5 * (both(0, h) + fb[i, rows].astype(F32))

    def final(h):
        rows = slice(h * HALF, (h + 1) * HALF)
        close(h, h).wait_recv()
        out_ref[rows, :] = (base_s[rows, :] + 0.5 * fb[h, rows].astype(F32)).astype(BF16)

    run("p4")
    with jax.named_scope("xn_forward"):
        xn_forward()
    with jax.named_scope("exchangelambdaipja"):
        exchange(lambda i: pj.at[i], lambda i: pr.at[i], pj_ss, pj_rs)
    with jax.named_scope("prtppjtp"):
        pr[tp] = pj[tp]
    run("p5")
    with jax.named_scope("xn_relayed_own"):
        xn_relayed((0,))
    run("p6")
    with jax.named_scope("xn_finish"):
        xn_finish()
    run("p7")
    with jax.named_scope("xn_relayed"):
        xn_relayed((3, 1))
    run("p8")
    with jax.named_scope("gate_up"):
        gate_up((0, 3, 1), "g")
    run("p9")
    with jax.named_scope("xn_relayed_far"):
        xn_relayed((2,))
    with jax.named_scope("gate_up_far"):
        gate_up((2,), "i")
    run("p12")
    with jax.named_scope("down2"):
        down(2, slice(0, HALF))
        half_to_partner(0).start()
        down(2, slice(HALF, ROWS))
        half_to_partner(1).start()
    with jax.named_scope("down1"):
        down(1)
        to_partner(1).start()
    with jax.named_scope("reduce_far"):
        reduce_far(0)
        reduce_far(1)
    with jax.named_scope("down3"):
        down(3)
        to_partner(3).start()
    with jax.named_scope("reduce_free0"):
        reduce_free(0)
    with jax.named_scope("reduce_free1"):
        reduce_free(1)
    with jax.named_scope("down0"):
        down(0)
        to_partner(0).start()
    with jax.named_scope("reduce_near0"):
        reduce_near(0)
    with jax.named_scope("reduce_near1"):
        reduce_near(1)
    with jax.named_scope("to_partner0wait_re"):
        to_partner(0).wait_recv()
    with jax.named_scope("exchangedlambdaipr"):
        exchanged(lambda i: pr.at[i], pj_ss, pj_rs)
    with jax.named_scope("begin"):
        begin(0)
        begin(1)
    with jax.named_scope("final0"):
        final(0)
    with jax.named_scope("final1"):
        final(1)

    with jax.named_scope("drain"):
        for name in pieces:
            drain(name)
    ref = kv.at[0, 0:15]
    copy(ref, ref, rel_ss, rel_rs.at[0], partner).wait_send()
    exchange_drain(lambda i: res_t.at[i], res_ss, res_rs)
    exchange_drain(lambda i: att_t.at[i], at_ss, at_rs)
    exchange_drain(lambda i: pr.at[i], pj_ss, pj_rs)
    wo_drain()
    xn_drain()
    for dx in (0, 1, 3):
        to_partner(dx).wait_send()
    for i in range(2):
        half_to_partner(i).wait_send()
        far(i).wait_send()
        close(i, 0).wait_send()
        close(i, 1).wait_send()


def on_device(residual_in, queries, keys, values, query_gain, key_norm_gain, out_weight, mlp_gain, gate_weight, up_weight, down_weight):
    tables = [jnp.asarray(t) for t in rotary_tables()]
    dma = pltpu.SemaphoreType.DMA
    vm = pltpu.VMEM
    scratch = [
        vm((2, 16, 6, 128, 128), BF16),
        vm((16, 128, 2 * FF_DEV), BF16),
        vm((16, 768, 128), BF16),
        vm((ROWS, HEAD), BF16),
        vm((8, TT, HEAD), BF16),
        vm((8, HEAD, D), BF16),
        vm((8, TT, 256), BF16),
        vm((TT, D), F32),
        vm((8, TT, D), BF16),
        vm((8, TT, 256), BF16),
        vm((8, TT, 256), BF16),
        vm((ROWS, 768), BF16),
        vm((4, 2, ROWS, 256), BF16),
        vm((4, ROWS, 256), BF16),
        vm((3, ROWS, 256), BF16),
        vm((2, HALF, 256), BF16),
        vm((2, ROWS, 256), BF16),
        vm((HEAD, ROWS), BF16),
        vm((1, ROWS), F32),
        vm((HEAD + 16, ROWS), F32),
        vm((2, ROWS, ROWS), F32),
        vm((2, 6 * TT, 256), F32),
        vm((ROWS, 256), F32),
        vm((ROWS, 256), BF16),
        vm((FF_DEV, HEAD), BF16),
        vm((FF_DEV, HEAD), BF16),
        pltpu.SemaphoreType.DMA((5,)),
        dma((2,)), dma((2, 16)), dma((6,)), dma((6, 16)), dma, dma((16,)),
        dma((2,)), dma((8,)), dma, dma((4,)), dma, dma((8,)), dma, dma((8,)),
        dma((2,)), dma((8,)), dma, dma((4,)), dma, dma((8,)),
        dma((5,)), dma((5,)), dma((2,)), dma((2,)), dma((2, 2)), dma((2, 2)),
    ]
    return pl.pallas_call(
        kernel,
        out_shape=jax.ShapeDtypeStruct((ROWS, 256), BF16),
        in_specs=[pl.BlockSpec(memory_space=pl.ANY if i in (0, 6, 8, 9, 10) else pltpu.VMEM) for i in range(15)],
        out_specs=pl.BlockSpec(memory_space=pltpu.VMEM),
        scratch_shapes=scratch,
        compiler_params=pltpu.CompilerParams(collective_id=0, has_side_effects=True, vmem_limit_bytes=60 * 1024 * 1024),
        name="layer",
    )(
        residual_in, queries, keys, values, query_gain.reshape(1, HEAD), key_norm_gain.reshape(1, HEAD), out_weight,
        mlp_gain.reshape(1, D), gate_weight.T, up_weight.T, down_weight, *tables,
    )


def solution(mesh):
    in_specs = (
        P("sp", "tp"), P("sp", "tp"), P("sp", None), P("sp", None), P(), P(), P("tp", None), P(),
        P("sp", "tp"), P("sp", "tp"), P("tp", "sp"),
    )
    return jax.shard_map(on_device, mesh=mesh, in_specs=in_specs, out_specs=P("sp", "tp"), check_vma=False)
```

time: 106 us -> 92.4 us (0.87)
  Pallas kernels: 103 us -> 90.5 us
    pallas_call x1, Pallas kernels: 103 us -> 90.5 us  [on_device(): pl.pallas_call(kernel, out_shape=jax.ShapeDtypeStruct((ROWS, 256), BF16),...]
where the time goes in v3:
time: 92.4 us; the launch traced here: 92.3 us
  Pallas kernels  90.5 us (98%)
  local copies, waits for them, and re-layouts  1.77 us (2%)
    pallas_call x1, Pallas kernels, on_device(): pl.pallas_call(kernel, out_shape=jax.ShapeDtypeStruct((ROWS, 256), BF16),...  90.5 us

profile of v3, /device:TPU:1, one launch (start us, length us, event | category | flops | bytes accessed | tf_op | source)
XLA Modules:
  0.0 92.3 jit_solution(10460337691963683826)
XLA Ops:
  0.0 90.5 %layer.1 = bf16[768,256]{1,0:T(8,128)(2,1)} custom-call(bf16[768,256]{1,0:T(8,128)(2,1)} %res_h.1, bf16[768,128]{1,0:T(8,128)(2,1)} %q_ref.1, bf16[768,256]{1,0:T(8,128)(2,1)} %k_ref.1, bf16[768,256]{1,0:T(8,128)(2,1)} %v_ref.1, f32[1,128]{1,0:T(1,128)} %bitcast.8, f32[1,128]{1,0:T(1,128)} %bitcast.9, bf16[128,2048]{1,0:T(8,128)(2,1)} %wo_h.1, ...), custom_call_target="tpu_custom_call" | custom-call | tf_op jit(solution)/shard_map/layer/pallas_call | solution.py:599
  90.5 1.8 %copy.17 = bf16[768,256]{1,0:T(8,128)(2,1)} copy(bf16[768,256]{1,0:T(8,128)(2,1)} %layer.1) | data formatting | bytes 786432

commit v4 on v3

--- a/solution.py
+++ b/solution.py
@@ -24,39 +24,42 @@
 F32 = jnp.float32
 BF16 = jnp.bfloat16
 
-ORDER = [(0, 0), (3, 0), (1, 0), (0, 1), (0, 3), (3, 3), (2, 0), (1, 3), (1, 1), (0, 2), (3, 1), (3, 2), (2, 3), (2, 1), (1, 2), (2, 2)]
+ORDER = [(0, 0), (0, 3), (1, 0), (0, 1), (3, 0), (0, 2), (1, 1), (2, 0), (1, 3), (3, 1), (3, 3), (1, 2), (2, 3), (2, 1), (3, 2), (2, 2)]
 SCHEDULE = {
-    "own": (("o", "gd", 1, 0), ("o", "gd", 0, 3),),
-    "a1": (("ka", 0, 3), ("ka", 3, 0), ("ka", 0, 1), ("ka", 1, 0), ("o", "ga", 3, 0), ("kb", 3, 0), ("r", 3, 0), ("kb", 1, 0), ("r", 1, 0), ("kb", 0, 1), ("r", 0, 1), ("kb", 0, 3), ("r", 0, 3),),
-    "a3": (("ka", 0, 2), ("ka", 1, 3), ("gd", 0, 1), ("gd", 3, 0),),
+    "own": (("o", "gd", 0, 3),),
+    "a1": (("o", "gd", 1, 0), ("ka", 0, 3), ("ka", 1, 0), ("ka", 3, 0), ("ka", 0, 1), ("o", "ga", 3, 0), ("kb", 0, 3), ("r", 0, 3), ("kb", 1, 0), ("r", 1, 0), ("kb", 0, 1), ("r", 0, 1), ("kb", 3, 0), ("r", 3, 0),),
+    "a3": (("ka", 0, 2), ("gd", 0, 1), ("gd", 3, 0), ("ka", 1, 3),),
     "a4": (("ka", 3, 3), ("ga", 0, 1),),
-    "a5": (("ka", 1, 1), ("kb", 3, 3), ("r", 3, 3), ("kb", 3, 1), ("ka", 2, 0), ("kb", 2, 0), ("r", 2, 0), ("kb", 1, 3), ("r", 1, 3),),
-    "a6": (("o", "gc", 0, 1),),
-    "a7": (("kb", 1, 1), ("r", 1, 1), ("kb", 0, 2), ("r", 0, 2), ("ka", 3, 1), ("r", 3, 1), ("ka", 1, 2), ("o", "gd", 0, 1),),
-    "a8": (("gd", 3, 1), ("ka", 3, 2), ("o", "ga", 1, 0),),
-    "a9": (("ka", 2, 3), ("gd", 3, 3), ("o", "gd", 3, 0),),
-    "a10": (("kb", 3, 2), ("r", 3, 2), ("ga", 3, 1), ("o", "gb", 3, 0), ("o", "gb", 1, 0),),
-    "a11": (("ga", 1, 1), ("kb", 2, 3), ("r", 2, 3),),
-    "a12": (("kb", 2, 1), ("gd", 0, 3), ("ka", 2, 1), ("r", 2, 1), ("gc", 3, 0), ("o", "gc", 3, 0),),
-    "a13": (("o", "ga", 0, 1), ("kb", 1, 2), ("r", 1, 2), ("ka", 2, 2), ("o", "ga", 0, 3), ("o", "gc", 1, 0),),
-    "a14": (("gd", 1, 0), ("ga", 0, 3),),
-    "a15": (("gb", 3, 0), ("kb", 2, 2), ("r", 2, 2), ("gb", 1, 0), ("gd", 3, 2),),
-    "p0": (("gc", 2, 0), ("ga", 2, 1), ("gc", 0, 1), ("gd", 0, 2),),
-    "p1": (("gd", 1, 1), ("ga", 3, 0), ("gc", 0, 3), ("ga", 1, 0),),
-    "p2": (("ga", 3, 3), ("gb", 3, 1), ("gd", 2, 0), ("gd", 1, 3), ("gb", 2, 0), ("gb", 1, 1), ("ga", 0, 2), ("ga", 1, 3), ("gc", 3, 1), ("gc", 0, 2), ("gb", 3, 3), ("gc", 1, 1),),
-    "p4": (("gd", 1, 2), ("ga", 2, 0), ("gb", 1, 3), ("gc", 1, 3), ("o", "gb", 0, 1), ("o", "db", 1, 0), ("gc", 3, 3), ("gb", 3, 2), ("o", "da", 3, 0), ("ga", 1, 2), ("gd", 2, 3), ("ga", 3, 2), ("gd", 2, 1), ("ga", 2, 3), ("gb", 2, 3), ("gc", 3, 2), ("gb", 2, 1), ("o", "gb", 0, 3), ("o", "gc", 0, 3), ("o", "db", 3, 0), ("gb", 0, 3), ("gc", 1, 2),),
-    "p5": (("o", "da", 1, 0), ("o", "db", 0, 1),),
-    "p6": (("db", 3, 0), ("gb", 1, 2), ("gc", 2, 1), ("gd", 2, 2), ("ga", 2, 2), ("da", 0, 1), ("o", "da", 0, 3), ("gb", 2, 2), ("gc", 2, 3),),
-    "p7": (("gc", 2, 2), ("gb", 0, 1), ("o", "da", 0, 1), ("gb", 0, 2), ("gc", 1, 0),),
-    "g0": (("o", "db", 0, 3),),
-    "g1": (("db", 2, 0), ("db", 1, 0), ("db", 3, 1), ("da", 0, 3),),
-    "g3": (("da", 0, 2), ("da", 3, 1), ("da", 1, 1), ("db", 0, 3),),
-    "p9": (("db", 0, 1), ("da", 3, 0),),
-    "i0": (("db", 3, 3), ("da", 1, 0),),
-    "p12": (("db", 2, 1), ("da", 3, 3), ("da", 1, 3), ("db", 2, 3), ("da", 3, 2), ("db", 1, 1), ("da", 1, 2), ("db", 1, 3), ("db", 3, 2), ("da", 2, 0), ("da", 2, 1), ("db", 0, 2), ("da", 2, 3), ("da", 2, 2), ("db", 2, 2), ("db", 1, 2),),
+    "a5": (("ka", 1, 1), ("kb", 0, 2), ("r", 0, 2), ("kb", 1, 1), ("r", 1, 1), ("ka", 2, 0), ("kb", 2, 0), ("r", 2, 0), ("kb", 1, 3), ("r", 1, 3),),
+    "a7": (("ka", 3, 1), ("ka", 1, 2), ("kb", 3, 1), ("r", 3, 1), ("kb", 3, 3), ("r", 3, 3), ("o", "gd", 0, 1), ("o", "gc", 0, 1),),
+    "a9": (("ka", 3, 2), ("gd", 3, 1), ("ka", 2, 3), ("gd", 3, 3), ("o", "gb", 3, 0), ("o", "gc", 1, 0),),
+    "a10": (("kb", 1, 2), ("r", 1, 2),),
+    "a11": (("kb", 2, 3), ("r", 2, 3), ("ga", 3, 1), ("ga", 1, 1), ("o", "gb", 1, 0),),
+    "a12": (("kb", 2, 1), ("gc", 3, 0), ("o", "gc", 3, 0),),
+    "a13": (("ka", 2, 1), ("r", 2, 1), ("gd", 0, 3), ("o", "gd", 3, 0), ("ka", 2, 2), ("kb", 3, 2), ("r", 3, 2), ("o", "ga", 0, 1), ("gc", 0, 3), ("o", "ga", 1, 0), ("gb", 1, 0),),
+    "a15": (("kb", 2, 2), ("r", 2, 2), ("gb", 3, 0), ("ga", 2, 1), ("gd", 3, 2), ("o", "gc", 0, 3),),
+    "p0": (("gc", 2, 0), ("gc", 0, 1), ("gd", 1, 0), ("gd", 0, 2),),
+    "p1": (("ga", 3, 0), ("ga", 0, 3), ("gb", 1, 1), ("gc", 1, 3),),
+    "p2": (("gc", 3, 3), ("gb", 3, 1), ("gb", 1, 3), ("gc", 1, 0), ("gb", 2, 0), ("gc", 0, 2), ("gb", 3, 3), ("gc", 1, 1), ("gd", 1, 1), ("gc", 3, 1), ("gd", 2, 0), ("gd", 1, 3),),
+    "p4": (("gb", 1, 2), ("ga", 2, 0), ("ga", 0, 2), ("ga", 1, 3), ("o", "dd", 1, 0), ("o", "gb", 0, 1), ("gb", 3, 2), ("ga", 3, 3), ("gb", 2, 3), ("gc", 2, 3), ("gb", 2, 1), ("gc", 3, 2), ("o", "da", 3, 0), ("gc", 1, 2), ("gd", 2, 3), ("ga", 3, 2), ("gd", 1, 2), ("o", "dc", 3, 0), ("o", "gb", 0, 3), ("gb", 0, 3), ("gc", 2, 1), ("o", "ga", 0, 3), ("o", "dc", 1, 0), ("o", "db", 1, 0), ("o", "da", 1, 0), ("o", "db", 3, 0), ("o", "dd", 0, 1), ("o", "dd", 3, 0), ("o", "dc", 0, 3),),
+    "p5": (("dd", 3, 0),),
+    "p6": (("gd", 2, 1), ("ga", 1, 2), ("gb", 2, 2), ("gc", 2, 2), ("da", 0, 1), ("o", "dd", 0, 3), ("o", "db", 0, 3), ("dc", 0, 1), ("o", "db", 0, 1), ("ga", 2, 3), ("gd", 2, 2), ("ga", 2, 2),),
+    "p7": (("gb", 0, 1), ("db", 3, 0), ("gb", 0, 2), ("ga", 1, 0), ("o", "da", 0, 1), ("o", "dc", 0, 1), ("o", "da", 0, 3),),
+    "g0": (("dd", 2, 0), ("dd", 3, 1), ("dc", 0, 3), ("db", 1, 0), ("da", 0, 2), ("da", 3, 1),),
+    "g1": (("dd", 1, 0), ("dc", 3, 1), ("dd", 0, 1), ("da", 0, 3),),
+    "g2": (("db", 0, 1), ("db", 2, 0), ("dc", 1, 0), ("dd", 0, 3), ("dd", 3, 3), ("da", 1, 1),),
+    "g3": (("dc", 0, 2), ("dc", 1, 1), ("da", 3, 0), ("db", 0, 3),),
+    "g4": (("db", 3, 3), ("dc", 3, 0), ("da", 1, 0), ("db", 3, 1), ("dc", 3, 3), ("dd", 2, 1),),
+    "p9": (("dc", 1, 3), ("dd", 2, 3), ("dd", 3, 2), ("da", 3, 2),),
+    "i0": (("da", 1, 2), ("db", 1, 3),),
+    "i1": (("da", 3, 3), ("db", 1, 1),),
+    "i2": (("da", 1, 3), ("dd", 1, 3),),
+    "i3": (("dc", 3, 2), ("dd", 1, 1),),
+    "i4": (("db", 2, 3), ("da", 2, 1),),
+    "p12": (("db", 2, 1), ("da", 2, 0), ("dc", 1, 2), ("dd", 0, 2), ("dc", 2, 0), ("db", 3, 2), ("db", 0, 2), ("dc", 2, 1), ("da", 2, 2), ("db", 1, 2), ("dc", 2, 3), ("dd", 2, 2), ("dc", 2, 2), ("dd", 1, 2), ("da", 2, 3), ("db", 2, 2),),
 }
 FAR_AT = 3
-MIRRORED = ("kb", "gc", "gd", "da")
+MIRRORED = ("kb", "gc", "gd", "da", "dc")
 
 
 def rotary_tables():
@@ -147,9 +150,9 @@
     pieces = {
         "ka": (lambda i: kv.at[core, i, 0:3], kv_ss.at[0], kv_rs.at[0]),
         "kb": (lambda i: kv.at[core, i, 3:6], kv_ss.at[1], kv_rs.at[1]),
-        "da": (lambda i: dn.at[i, 0:352], w_ss.at[4], w_rs.at[4]),
-        "db": (lambda i: dn.at[i, 352:704], w_ss.at[5], w_rs.at[5]),
     }
+    for n, name in enumerate(("da", "db", "dc", "dd")):
+        pieces[name] = (lambda i, n=n: dn.at[i, n * 176 : (n + 1) * 176], w_ss.at[4 + n], w_rs.at[4 + n])
     for n, name in enumerate(("ga", "gb", "gc", "gd")):
         pieces[name] = (lambda i, n=n: gu.at[i, n * 32 : (n + 1) * 32], w_ss.at[n], w_rs.at[n])
 
@@ -591,7 +594,7 @@
         vm((FF_DEV, HEAD), BF16),
         vm((FF_DEV, HEAD), BF16),
         pltpu.SemaphoreType.DMA((5,)),
-        dma((2,)), dma((2, 16)), dma((6,)), dma((6, 16)), dma, dma((16,)),
+        dma((2,)), dma((2, 16)), dma((8,)), dma((8, 16)), dma, dma((16,)),
         dma((2,)), dma((8,)), dma, dma((4,)), dma, dma((8,)), dma, dma((8,)),
         dma((2,)), dma((8,)), dma, dma((4,)), dma, dma((8,)),
         dma((5,)), dma((5,)), dma((2,)), dma((2,)), dma((2, 2)), dma((2, 2)),

time: 92.4 us -> 94.1 us (1.018)
  Pallas kernels: 90.5 us -> 92.2 us
    pallas_call x1, Pallas kernels: 90.5 us -> 92.2 us  [on_device(): pl.pallas_call(kernel, out_shape=jax.ShapeDtypeStruct((ROWS, 256), BF16),...]
where the time goes in v4:
time: 94.1 us; the launch traced here: 94 us
  Pallas kernels  92.2 us (98%)
  local copies, waits for them, and re-layouts  1.77 us (2%)
    pallas_call x1, Pallas kernels, on_device(): pl.pallas_call(kernel, out_shape=jax.ShapeDtypeStruct((ROWS, 256), BF16),...  92.2 us

profile of v4, /device:TPU:1, one launch (start us, length us, event | category | flops | bytes accessed | tf_op | source)
XLA Modules:
  0.0 94.0 jit_solution(318122171928869155)
XLA Ops:
  0.0 92.2 %layer.1 = bf16[768,256]{1,0:T(8,128)(2,1)} custom-call(bf16[768,256]{1,0:T(8,128)(2,1)} %res_h.1, bf16[768,128]{1,0:T(8,128)(2,1)} %q_ref.1, bf16[768,256]{1,0:T(8,128)(2,1)} %k_ref.1, bf16[768,256]{1,0:T(8,128)(2,1)} %v_ref.1, f32[1,128]{1,0:T(1,128)} %bitcast.8, f32[1,128]{1,0:T(1,128)} %bitcast.9, bf16[128,2048]{1,0:T(8,128)(2,1)} %wo_h.1, ...), custom_call_target="tpu_custom_call" | custom-call | tf_op jit(solution)/shard_map/layer/pallas_call | solution.py:602
  92.2 1.8 %copy.17 = bf16[768,256]{1,0:T(8,128)(2,1)} copy(bf16[768,256]{1,0:T(8,128)(2,1)} %layer.1) | data formatting | bytes 786432
